TPU v7x, 32 devices: a whole 2x2x4 slice. The times are simulated.
32 devices in a mesh: gr: 2 (over x), fs: 4 (over z), tp: 4 (over y, core).
Axes of the slice: x: 2, y: 2, z: 4, core: 2. Of those that a mesh axis runs over, the one named last changes fastest.
Arguments:
- prompt: bfloat16 [4096, 2048], P(('gr', 'fs', 'tp')), may hold values from -6 to 6
- train_gate: float32 [16, 2048, 256], P(None, ('gr', 'fs'), 'tp'), may hold values from -0.125 to 0.125
- train_up: float32 [16, 2048, 256], P(None, ('gr', 'fs'), 'tp'), may hold values from -0.125 to 0.125
- train_down: float32 [16, 256, 2048], P(None, 'tp', ('gr', 'fs')), may hold values from -0.375 to 0.375
- train_shared_gate: float32 [2048, 256], P(('gr', 'fs'), 'tp'), may hold values from -0.125 to 0.125
- train_shared_up: float32 [2048, 256], P(('gr', 'fs'), 'tp'), may hold values from -0.125 to 0.125
- train_shared_down: float32 [256, 2048], P('tp', ('gr', 'fs')), may hold values from -0.375 to 0.375
- norm_gain: float32 [2048], P(('gr', 'fs')), may hold values from 0.1 to 1.9
- expert_ids: int32 [4096, 8], P(('gr', 'fs', 'tp')), may hold values from 0 to 15, all different within a row; in each aligned block of 128 rows (0 to 127, 128 to 255, ...) at most 65 rows name the same one
- route_weight: float32 [4096, 8], P(('gr', 'fs', 'tp')), may hold values from 0.05 to 0.6
Outputs:
- serve_gate: bfloat16 [16, 2048, 256], P(('fs', 'tp'))
- serve_up: bfloat16 [16, 2048, 256], P(('fs', 'tp'))
- serve_down: bfloat16 [16, 256, 2048], P(('fs', 'tp'))
- serve_shared_gate: bfloat16 [2048, 256], P(None, 'tp')
- serve_shared_up: bfloat16 [2048, 256], P(None, 'tp')
- serve_shared_down: bfloat16 [256, 2048], P('tp')
- mixed_out: bfloat16 [4096, 2048], P(('gr', 'fs', 'tp'))
Inputs may be any that keep to these rules, and one draw needn't show every extreme that they name: `expert_ids`: each row names 8 different experts. Among the rows of one device no expert is named by more than 65 rows, and in some device's rows one expert is named by exactly 65.
All inputs are finite; a program needn't handle non-finite values.
Results may differ from a plain program's by a relative error of at most 0.012.
Values may be sent and summed in bfloat16 or wider, within the bound.
A program may use at most 128 MiB of HBM per device.

v0:
```python
import functools

import jax
import jax.numpy as jnp
from jax import lax
from jax.experimental import pallas as pl
from jax.experimental.pallas import tpu as pltpu
from jax.sharding import PartitionSpec as P

eps_norm = 1e-06
MESH = pl.DeviceIdType.MESH
CORES = 2
VMEM_PLAN = 40 * 2**20
VMEM_LIMIT = 60 * 2**20


def plane_kernel(
    n_gr, n_fs, n_tp, parts,
    p_ref, gt_ref, ut_ref, dn_ref, sg_ref, su_ref, sd_ref, gain_ref, ids_ref, rw_ref,
    gate_hbm, up_hbm, down_hbm, sg_hbm, su_hbm, sd_hbm, mixed_out,
    x_in, w_in, e_in, s_in, gate_out, up_out, down_out, s_out,
    x_all, w_all, e_all, s_gu, part, rc, ry, ru, rd, sh,
    xr, wr, er, sr, zs, ys, cs, as_, fs_sem, ss, loc,
    ks, kr, qs, qr, us, ur, ds_, dr, res_sem,
):
    gr, z, tp = lax.axis_index("gr"), lax.axis_index("fs"), lax.axis_index("tp")
    y, c = tp // CORES, tp % CORES
    y_peer = (1 - y) * CORES + c
    c_peer = y * CORES + 1 - c
    x_peer = 1 - gr
    plane = n_fs * n_tp
    _, hid, cols_d = s_in.shape
    sub, width = x_in.shape[1], x_in.shape[2]
    rows = parts * sub

    def dev(g, f, t):
        return {"gr": g, "fs": f, "tp": t}

    peers = [
        (dz, dt, (z + dz) % n_fs, (tp + dt) % n_tp)
        for dz in range(n_fs)
        for dt in range(n_tp)
        if dz or dt
    ]
    barrier = pltpu.get_barrier_semaphore()
    for _, _, f, t in peers:
        pl.semaphore_signal(barrier, inc=1, device_id=dev(gr, f, t), device_id_type=MESH)
    pl.semaphore_signal(barrier, inc=1, device_id=dev(x_peer, z, tp), device_id_type=MESH)

    gain = gain_ref[...]

    def cast(i, carry):
        e_in[i, 0] = (gt_ref[i] * gain).astype(jnp.bfloat16)
        e_in[i, 1] = (ut_ref[i] * gain).astype(jnp.bfloat16)
        e_in[i, 2] = dn_ref[i].astype(jnp.bfloat16)
        return carry

    s_in[0] = (sg_ref[...] * gain).astype(jnp.bfloat16)
    s_in[1] = (su_ref[...] * gain).astype(jnp.bfloat16)
    s_in[2] = sd_ref[...].astype(jnp.bfloat16)
    for h in range(parts):
        v = p_ref[h * sub : (h + 1) * sub, :].astype(jnp.float32)
        mean = jnp.mean(v * v, axis=-1, keepdims=True)
        x_in[h] = (v * lax.rsqrt(mean + eps_norm)).astype(jnp.bfloat16)
    table = jnp.zeros(w_in.shape, jnp.float32)
    which = lax.broadcasted_iota(jnp.int32, w_in.shape, 0)
    for k in range(ids_ref.shape[0]):
        table = table + jnp.where(ids_ref[k : k + 1, :] == which, rw_ref[k : k + 1, :], 0.0)
    w_in[...] = table
    lax.fori_loop(0, plane, cast, 0)
    pl.semaphore_wait(barrier, plane)

    def remote(src, dst, send, recv, where):
        return pltpu.make_async_remote_copy(
            src_ref=src, dst_ref=dst, send_sem=send, recv_sem=recv,
            device_id=where, device_id_type=MESH,
        )

    def cols_of(g, f):
        return pl.ds(pl.multiple_of((g * n_fs + f) * cols_d, 128), cols_d)

    def e_at(g, f, t):
        return e_all.at[g * n_fs + f, t]

    def s_at(g, f):
        return s_out.at[:, :, cols_of(g, f)]

    def block(src_own, owner, sems, slot, where, h):
        xs = x_in.at[h] if src_own else x_all.at[owner, h]
        copies = [remote(xs, x_all.at[owner, h], sems.at[slot, h], xr.at[owner, h], where)]
        if h == 0:
            ws = w_in if src_own else w_all.at[owner]
            copies.append(remote(ws, w_all.at[owner], sems.at[slot, parts], wr.at[owner], where))
        return copies

    def shared(src_own, g, f, slot, where):
        src = s_in if src_own else s_at(g, f)
        return [remote(src, s_at(g, f), ss.at[slot], sr.at[g * n_fs + f], where)]

    def expert(src_own, f, t, slot):
        src = e_in.at[z * n_tp + tp] if src_own else e_at(gr, f, t)
        k = gr * plane + f * n_tp + t
        return [remote(src, e_at(gr, f, t), fs_sem.at[slot], er.at[k], dev(x_peer, z, tp))]

    own = tp * n_fs + z
    up, down = dev(gr, z + 1, tp), dev(gr, z - 1, tp)
    has_up, has_down = z < n_fs - 1, z > 0
    to_y, to_c, to_x = dev(gr, z, y_peer), dev(gr, z, c_peer), dev(x_peer, z, tp)
    pending = []

    def start(copies):
        for one in copies:
            one.start()

    def go(cond, copies):
        pending.append((cond, copies))
        if cond is None:
            start(copies)
        else:
            pl.when(cond)(lambda: start(copies))

    for h in range(parts):
        go(has_up, block(True, own, zs, 0, up, h))
        go(has_down, block(True, own, zs, 1, down, h))
        go(None, block(True, own, ys, 0, to_y, h))
        go(None, block(True, own, cs, 0, to_c, h))
    go(None, expert(True, z, tp, 0))
    go(has_up, shared(True, gr, z, 1, up))
    go(has_down, shared(True, gr, z, 2, down))
    go(None, shared(True, gr, z, 0, to_x))
    locals_ = [
        pltpu.make_async_copy(x_in, x_all.at[own], loc.at[0]),
        pltpu.make_async_copy(w_in, w_all.at[own], loc.at[1]),
        pltpu.make_async_copy(e_in.at[z * n_tp + tp], e_at(gr, z, tp), loc.at[2]),
        pltpu.make_async_copy(s_in, s_at(gr, z), loc.at[3]),
    ]
    start(locals_)

    def send_experts(want):
        for dz, dt, f, t in peers:
            if dz == want:
                mine = gr * plane + z * n_tp + tp
                go(None, [remote(
                    e_in.at[f * n_tp + t], e_at(gr, z, tp),
                    as_.at[dz * n_tp + dt], er.at[mine], dev(gr, f, t),
                )])

    def wait_expert(g, f, t):
        k = g * plane + f * n_tp + t
        remote(e_in.at[0], e_at(g, f, t), as_.at[0], er.at[k], to_x).wait_recv()

    def wait_block(owner, h):
        for one in block(True, owner, cs, 0, to_c, h):
            one.wait_recv()

    def wait_shared(g, f):
        shared(True, g, f, 0, to_x)[0].wait_recv()

    def pass_experts(want):
        for dz, dt, _, _ in peers:
            if dz == want:
                f, t = (z + n_fs - dz) % n_fs, (tp + n_tp - dt) % n_tp
                wait_expert(gr, f, t)
                go(None, expert(False, f, t, dz * n_tp + dt))

    send_experts(0)
    send_experts(1)
    for d in range(1, n_fs):
        for h in range(parts):
            for way in (0, 1):
                f = z - d if way == 0 else z + d
                there = f >= 0 if way == 0 else f < n_fs
                more = has_up if way == 0 else has_down
                onward = up if way == 0 else down
                owner = tp * n_fs + f
                slot = 2 * d + way
                pl.when(there)(functools.partial(wait_block, owner, h))
                go(there & more, block(False, owner, zs, slot, onward, h))
                go(there, block(False, owner, ys, slot, to_y, h))
                go(there, block(False, owner, cs, slot, to_c, h))
                if h == parts - 1:
                    pl.when(there)(functools.partial(wait_shared, gr, f))
                    go(there & more, shared(False, gr, f, 2 * slot + 1, onward))
                    go(there, shared(False, gr, f, 2 * slot, to_x))
        if d + 1 < n_fs:
            send_experts(d + 1)
        pass_experts(d - 1)
    pass_experts(n_fs - 1)
    for k in range(n_fs):
        f = (z + k) % n_fs
        owner = y_peer * n_fs + f
        for h in range(parts):
            wait_block(owner, h)
            go(None, block(False, owner, cs, 2 * n_fs + k, to_c, h))
    for f in range(n_fs):
        for t in range(n_tp):
            wait_expert(x_peer, f, t)
        wait_shared(x_peer, f)
        for yy in range(n_tp // CORES):
            for h in range(parts):
                wait_block((yy * CORES + 1 - c) * n_fs + f, h)
    for one in locals_:
        one.wait()

    def turn(k, carry):
        here = pl.ds(pl.multiple_of(k * cols_d, 128), cols_d)
        gate_out[here, :] = e_all[k, :, 0].reshape(n_tp * hid, cols_d).T
        up_out[here, :] = e_all[k, :, 1].reshape(n_tp * hid, cols_d).T
        down_out[:, here] = e_all[k, :, 2].reshape(n_tp * hid, cols_d)
        s_gu[here, :] = s_out[0:2, :, here].reshape(2 * hid, cols_d).T
        return carry

    lax.fori_loop(0, n_gr * n_fs, turn, 0)
    results = [
        pltpu.make_async_copy(src, dst, res_sem.at[i])
        for i, (src, dst) in enumerate((
            (gate_out, gate_hbm), (up_out, up_hbm), (down_out, down_hbm),
            (s_out.at[0], sg_hbm), (s_out.at[1], su_hbm), (s_out.at[2], sd_hbm),
        ))
    ]
    start(results)

    step = 2
    chunk = min(width, 512)
    me = z * n_tp + tp

    def compute(group):
        def rows_of(k, carry):
            first = group * n_fs + k * step
            xs = x_all[pl.ds(first, step)].reshape(step * rows, width)
            ws = jnp.concatenate(
                [
                    jnp.broadcast_to(w_all[first + i, pl.ds(me, 1), :], (rows, rows)).T[:, :1]
                    for i in range(step)
                ],
                axis=0,
            )
            gate = jnp.dot(xs, gate_out[...], preferred_element_type=jnp.float32)
            upv = jnp.dot(xs, up_out[...], preferred_element_type=jnp.float32)
            act = (jax.nn.silu(gate) * upv * ws).astype(jnp.bfloat16)
            sh[...] = jnp.zeros_like(sh)

            @pl.when(z // step == k)
            def _():
                both = jnp.dot(
                    x_all[group * n_fs + z].reshape(rows, width), s_gu[...],
                    preferred_element_type=jnp.float32,
                )
                val = jax.nn.silu(both[:, :hid]) * both[:, hid:]
                sh[pl.ds(pl.multiple_of((z % step) * rows, 128), rows), :] = val.astype(jnp.bfloat16)

            extra = sh[...]

            def cols(j, inner):
                at = pl.ds(pl.multiple_of(j * chunk, 128), chunk)
                res = jnp.dot(act, down_out[:, at], preferred_element_type=jnp.float32)
                res = res + jnp.dot(extra, s_out[2, :, at], preferred_element_type=jnp.float32)
                part[pl.ds(first, step), :, :, at] = res.astype(jnp.bfloat16).reshape(
                    step, parts, sub, chunk
                )
                return inner

            return lax.fori_loop(0, width // chunk, cols, carry)

        lax.fori_loop(0, n_fs // step, rows_of, 0)

    other_y, other_c = 1 - y, 1 - c
    g_y = y_peer
    g_own = tp

    def wide(v):
        return v.astype(jnp.float32)

    def c_copy(i):
        group = (other_y if i == 0 else y) * CORES + other_c
        return remote(part.at[pl.ds(group * n_fs, n_fs)], rc.at[i], ks.at[i], kr.at[i], to_c)

    spots = []
    for d in range(n_fs - 1, -1, -1):
        for way in (0, 1):
            if d == 0 and way == 1:
                continue
            t = z + d if way == 0 else z - d
            spots.append((d, way, t, (t < n_fs) if way == 0 else (t >= 0)))

    def y_copy(t, h):
        return remote(part.at[g_y * n_fs + t, h], ry.at[t, h], qs.at[t, h], qr.at[t, h], to_y)

    def u_copy(t, h):
        return remote(part.at[g_own * n_fs + t, h], ru.at[t, h], us.at[t, h], ur.at[t, h], up)

    def d_copy(t, h):
        return remote(part.at[g_own * n_fs + t, h], rd.at[t, h], ds_.at[t, h], dr.at[t, h], down)

    def phase(i, carry):
        gy = jnp.where(i == 0, other_y, y)

        def one(k, inner):
            compute(gy * CORES + jnp.where(k == 0, other_c, c))

            @pl.when(k == 0)
            def _():
                pl.when(i == 0)(lambda: c_copy(0).start())
                pl.when(i == 1)(lambda: c_copy(1).start())

            return inner

        lax.fori_loop(0, 2, one, 0)

        @pl.when(i == 0)
        def _():
            c_copy(0).wait_recv()
            for _d, _way, t, there in spots:

                @pl.when(there)
                def _(t=t):
                    for h in range(parts):
                        at = g_y * n_fs + t
                        part[at, h] = (wide(part[at, h]) + wide(rc[0, t, h])).astype(jnp.bfloat16)
                        y_copy(t, h).start()

        return carry

    lax.fori_loop(0, 2, phase, 0)
    c_copy(1).wait_recv()

    for d, way, t, there in spots:

        @pl.when(there)
        def _(d=d, way=way, t=t):
            at = g_own * n_fs + t
            for h in range(parts):
                y_copy(t, h).wait_recv()
                total = wide(part[at, h]) + wide(rc[1, t, h]) + wide(ry[t, h])
                if d == 0:
                    mixed_out[h] = total.astype(jnp.bfloat16)

                    @pl.when(has_down & has_up)
                    def _():
                        u_copy(t, h).wait_recv()
                        d_copy(t, h).wait_recv()
                        mixed_out[h] = (total + wide(ru[t, h]) + wide(rd[t, h])).astype(jnp.bfloat16)

                    @pl.when(has_down & jnp.logical_not(has_up))
                    def _():
                        u_copy(t, h).wait_recv()
                        mixed_out[h] = (total + wide(ru[t, h])).astype(jnp.bfloat16)

                    @pl.when(has_up & jnp.logical_not(has_down))
                    def _():
                        d_copy(t, h).wait_recv()
                        mixed_out[h] = (total + wide(rd[t, h])).astype(jnp.bfloat16)
                else:
                    copy, arrived, before = (
                        (u_copy, ru, has_down) if way == 0 else (d_copy, rd, has_up)
                    )
                    part[at, h] = total.astype(jnp.bfloat16)

                    @pl.when(before)
                    def _():
                        copy(t, h).wait_recv()
                        part[at, h] = (total + wide(arrived[t, h])).astype(jnp.bfloat16)

                    copy(t, h).start()

    for one in results:
        one.wait()
    for cond, copies in pending:
        if cond is None:
            for one in copies:
                one.wait_send()
        else:

            @pl.when(cond)
            def _(copies=copies):
                for one in copies:
                    one.wait_send()
    c_copy(0).wait_send()
    c_copy(1).wait_send()
    for d, way, t, there in spots:

        @pl.when(there)
        def _(d=d, way=way, t=t):
            for h in range(parts):
                y_copy(t, h).wait_send()
                if d:
                    (u_copy if way == 0 else d_copy)(t, h).wait_send()


def small_body(
    n_gr, n_fs, n_tp,
    prompt, train_gate, train_up, train_down, train_shared_gate, train_shared_up,
    train_shared_down, norm_gain, expert_ids, route_weight,
):
    experts, rows_d, hid = train_gate.shape
    rows, width = prompt.shape
    plane, full, parts = n_fs * n_tp, n_gr * n_fs, 2
    sub = rows // parts
    bf16 = jnp.bfloat16
    vmem = pl.BlockSpec(memory_space=pltpu.VMEM)
    dma = pltpu.SemaphoreType.DMA
    shape = jax.ShapeDtypeStruct
    serve_gate, serve_up, serve_down, s_gate, s_up, s_down, mixed_out = pl.pallas_call(
        functools.partial(plane_kernel, n_gr, n_fs, n_tp, parts),
        out_shape=(
            shape((width, n_tp * hid), bf16),
            shape((width, n_tp * hid), bf16),
            shape((n_tp * hid, width), bf16),
            shape((hid, width), bf16),
            shape((hid, width), bf16),
            shape((hid, width), bf16),
            shape((parts, sub, width), bf16),
        ),
        in_specs=[vmem] * 10,
        out_specs=(pl.BlockSpec(memory_space=pl.ANY),) * 6 + (vmem,),
        scratch_shapes=[
            pltpu.VMEM((parts, sub, width), bf16),
            pltpu.VMEM((experts, rows), jnp.float32),
            pltpu.VMEM((experts, 3, hid, rows_d), bf16),
            pltpu.VMEM((3, hid, rows_d), bf16),
            pltpu.VMEM((width, n_tp * hid), bf16),
            pltpu.VMEM((width, n_tp * hid), bf16),
            pltpu.VMEM((n_tp * hid, width), bf16),
            pltpu.VMEM((3, hid, width), bf16),
            pltpu.VMEM((plane, parts, sub, width), bf16),
            pltpu.VMEM((plane, experts, rows), jnp.float32),
            pltpu.VMEM((full, n_tp, 3, hid, width // full), bf16),
            pltpu.VMEM((width, 2 * hid), bf16),
            pltpu.VMEM((plane, parts, sub, width), bf16),
            pltpu.VMEM((2, n_fs, parts, sub, width), bf16),
            pltpu.VMEM((n_fs, parts, sub, width), bf16),
            pltpu.VMEM((n_fs, parts, sub, width), bf16),
            pltpu.VMEM((n_fs, parts, sub, width), bf16),
            pltpu.VMEM((2 * rows, hid), bf16),
            dma((plane, parts)), dma((plane,)), dma((n_gr * plane,)), dma((full,)),
            dma((2 * n_fs, parts + 1)), dma((2 * n_fs, parts + 1)), dma((3 * n_fs, parts + 1)),
            dma((plane,)), dma((plane,)), dma((4 * n_fs,)), dma((4,)),
            dma((2,)), dma((2,)),
            dma((n_fs, parts)), dma((n_fs, parts)), dma((n_fs, parts)),
            dma((n_fs, parts)), dma((n_fs, parts)), dma((n_fs, parts)), dma((6,)),
        ],
        compiler_params=pltpu.CompilerParams(
            collective_id=0, has_side_effects=True, vmem_limit_bytes=VMEM_LIMIT
        ),
    )(
        prompt, train_gate.transpose(0, 2, 1), train_up.transpose(0, 2, 1), train_down,
        train_shared_gate.T, train_shared_up.T, train_shared_down, norm_gain[None, :],
        expert_ids.T, route_weight.T,
    )
    return (
        serve_gate[None], serve_up[None], serve_down[None],
        s_gate.T, s_up.T, s_down, mixed_out.reshape(rows, width),
    )


def regroup(stacked, lowered):
    stacked = lax.all_to_all(
        lax.all_to_all(stacked, "fs", split_axis=0, concat_axis=2, tiled=True),
        "tp",
        split_axis=0,
        concat_axis=3,
        tiled=True,
    )
    lowered = lax.all_to_all(
        lax.all_to_all(lowered, "fs", split_axis=0, concat_axis=2, tiled=True),
        "tp",
        split_axis=0,
        concat_axis=1,
        tiled=True,
    )
    return (stacked, lowered)


def body(
    prompt,
    train_gate,
    train_up,
    train_down,
    train_shared_gate,
    train_shared_up,
    train_shared_down,
    norm_gain,
    expert_ids,
    route_weight,
):
    gain_col = norm_gain[:, None]
    stacked = jnp.stack((train_gate * gain_col[None], train_up * gain_col[None]), axis=1).astype(
        jnp.bfloat16
    )
    lowered = train_down.astype(jnp.bfloat16)
    stacked, lowered = regroup(stacked, lowered)
    stacked, lowered = (
        lax.all_gather(stacked, "gr", axis=2, tiled=True),
        lax.all_gather(lowered, "gr", axis=2, tiled=True),
    )
    serve_gate = stacked[:, 0]
    serve_up = stacked[:, 1]
    serve_shared_gate, serve_shared_up, serve_shared_down = (
        lax.all_gather(
            (train_shared_gate * gain_col).astype(jnp.bfloat16), ("gr", "fs"), axis=0, tiled=True
        ),
        lax.all_gather(
            (train_shared_up * gain_col).astype(jnp.bfloat16), ("gr", "fs"), axis=0, tiled=True
        ),
        lax.all_gather(train_shared_down.astype(jnp.bfloat16), ("gr", "fs"), axis=1, tiled=True),
    )
    widened = prompt.astype(jnp.float32)
    normed = (
        widened * lax.rsqrt(jnp.mean(widened * widened, axis=-1, keepdims=True) + eps_norm)
    ).astype(jnp.bfloat16)
    block_rows = lax.all_gather(normed, "tp", axis=0, tiled=True)
    gate_val = jnp.dot(block_rows, serve_shared_gate, preferred_element_type=jnp.float32)
    up_val = jnp.dot(block_rows, serve_shared_up, preferred_element_type=jnp.float32)
    shared_act = (jax.nn.silu(gate_val) * up_val).astype(jnp.bfloat16)
    shared_sum = lax.psum_scatter(
        jnp.dot(shared_act, serve_shared_down, preferred_element_type=jnp.float32).astype(
            jnp.bfloat16
        ),
        "tp",
        scatter_dimension=0,
        tiled=True,
    ).astype(jnp.float32)
    row_count = prompt.shape[0]
    top_count = expert_ids.shape[1]
    model_width = prompt.shape[1]
    expert_count = lax.axis_size("fs") * lax.axis_size("tp")
    capacity = row_count * top_count // expert_count + 1
    flat_ids = expert_ids.reshape(-1)
    onehot = (flat_ids[:, None] == jnp.arange(expert_count, dtype=jnp.int32)[None, :]).astype(
        jnp.int32
    )
    earlier = jnp.cumsum(onehot, axis=0) - onehot
    places = jnp.sum(earlier * onehot, axis=1)
    slot_ids = (flat_ids * capacity + places).reshape(row_count, top_count)
    slot_range = jnp.arange(expert_count * capacity, dtype=jnp.int32)
    dispatch = jnp.any(slot_range[:, None, None] == slot_ids[None, :, :], axis=-1).astype(
        jnp.bfloat16
    )
    outgoing = jnp.dot(dispatch, normed, preferred_element_type=jnp.float32).astype(jnp.bfloat16)
    outgoing = outgoing.reshape(expert_count, capacity, model_width)
    arrived = lax.all_to_all(outgoing, ("fs", "tp"), split_axis=0, concat_axis=0, tiled=True)
    source_count, slot_count, width_here = arrived.shape
    arrived_rows = arrived.reshape(source_count * slot_count, width_here)
    gate_val = jnp.dot(arrived_rows, serve_gate[0], preferred_element_type=jnp.float32)
    up_val = jnp.dot(arrived_rows, serve_up[0], preferred_element_type=jnp.float32)
    hidden = (jax.nn.silu(gate_val) * up_val).astype(jnp.bfloat16)
    result = jnp.dot(hidden, lowered[0], preferred_element_type=jnp.float32).astype(jnp.bfloat16)
    result = result.reshape(source_count, slot_count, width_here)
    returned = lax.all_to_all(result, ("fs", "tp"), split_axis=0, concat_axis=0, tiled=True)
    picked = returned.reshape(expert_count * capacity, model_width)[slot_ids]
    routed = jnp.sum(route_weight[:, :, None] * picked.astype(jnp.float32), axis=1)
    mixed_out = (routed + shared_sum).astype(jnp.bfloat16)
    return (
        serve_gate,
        serve_up,
        lowered,
        serve_shared_gate,
        serve_shared_up,
        serve_shared_down,
        mixed_out,
    )


def solution(mesh):
    placed = (
        P(("gr", "fs", "tp"), None),
        P(None, ("gr", "fs"), "tp"),
        P(None, ("gr", "fs"), "tp"),
        P(None, "tp", ("gr", "fs")),
        P(("gr", "fs"), "tp"),
        P(("gr", "fs"), "tp"),
        P("tp", ("gr", "fs")),
        P(("gr", "fs")),
        P(("gr", "fs", "tp"), None),
        P(("gr", "fs", "tp"), None),
    )
    n_gr, n_fs, n_tp = (mesh.shape[name] for name in ("gr", "fs", "tp"))

    def chosen(prompt, *rest):
        held = n_fs * n_tp * prompt.size * prompt.dtype.itemsize * 5 // 2
        if n_gr == 2 and n_tp == 2 * CORES and n_fs % 2 == 0 and held < VMEM_PLAN:
            return small_body(n_gr, n_fs, n_tp, prompt, *rest)
        return body(prompt, *rest)

    return jax.shard_map(
        chosen,
        mesh=mesh,
        in_specs=placed,
        out_specs=(
            P(("fs", "tp"), None, None),
            P(("fs", "tp"), None, None),
            P(("fs", "tp"), None, None),
            P(None, "tp"),
            P(None, "tp"),
            P("tp", None),
            P(("gr", "fs", "tp"), None),
        ),
        check_vma=False,
    )
```

profile of v0, /device:TPU:24, one launch (start us, length us, event | category | flops | bytes accessed | tf_op | source)
XLA Modules:
  0.0 163.4 jit_solution(2169920224540976721)
XLA Ops:
  0.6 154.5 %shard_map.153 = (bf16[2048,256]{1,0:T(8,128)(2,1)}, bf16[2048,256]{1,0:T(8,128)(2,1)}, bf16[256,2048]{1,0:T(8,128)(2,1)}, bf16[64,2048]{1,0:T(8,128)(2,1)}, bf1...) custom-call(bf16[128,2048]{1,0:T(8,128)(2,1)} %p_ref.1, f32[16,64,256]{2,1,0:T(8,128)} %bitcast.16, ...), custom_call_target="tpu_custom_call" | custom-call | tf_op jit(solution)/shard_map/pallas_call | solution.py:403
  155.1 0.0 copy-start.1
  155.1 2.4 %copy.24 = bf16[1,2048,256]{2,1,0:T(8,128)(2,1)} copy(bf16[1,2048,256]{2,1,0:T(8,128)(2,1)} %bitcast.15) | data formatting | bytes 2097152
  157.5 0.0 copy-done.1
  157.5 0.0 copy-start
  157.5 1.0 copy.25
  158.4 0.6 copy-done
  159.1 0.0 copy-start.5
  159.1 1.0 copy.26
  160.0 0.1 copy-done.5
  160.2 0.0 copy-start.4
  160.2 0.0 copy-start.3
  160.2 0.7 copy.27
  160.9 0.3 copy-done.4
  161.2 0.0 copy-start.2
  161.2 0.7 copy.28
  161.9 0.0 copy-done.3
  161.9 0.7 copy.29
  162.6 0.0 copy-done.2
  162.6 0.8 copy.30
Async XLA Ops:
  155.1 2.4 %copy-start.1 = (bf16[2048,256]{1,0:T(8,128)(2,1)S(1)}, bf16[2048,256]{1,0:T(8,128)(2,1)}, u32[]{:S(2)}) copy-start(bf16[2048,256]{1,0:T(8,128)(2,1)} %get-tuple-element.15) | copy-start | bytes 3145732
  157.5 1.6 copy-start
  159.1 1.1 copy-start.5
  160.2 1.0 copy-start.4
  160.2 1.7 %copy-start.3 = (bf16[64,2048]{1,0:T(8,128)(2,1)S(1)}, bf16[64,2048]{1,0:T(8,128)(2,1)}, u32[]{:S(2)}) copy-start(bf16[64,2048]{1,0:T(8,128)(2,1)} %get-tuple-element.33) | copy-start | bytes 786436
  161.2 1.4 copy-start.2
where the time goes:
time: 164 us; the launch traced here: 163 us
  Pallas kernels  154 us (94%)
  local copies, waits for them, and re-layouts  8.29 us (5%)
    pallas_call x1, Pallas kernels, small_body(): pl.pallas_call(functools.partial(plane_kernel, n_gr, n_fs, n_tp, parts),...  154 us
    unnamed x19, local copies, waits for them, and re-layouts  8.29 us

commit v1 on v0

v1 whole, which is shorter than its diff:
```python
import functools

import jax
import jax.numpy as jnp
from jax import lax
from jax.experimental import pallas as pl
from jax.experimental.pallas import tpu as pltpu
from jax.sharding import PartitionSpec as P

eps_norm = 1e-06
MESH = pl.DeviceIdType.MESH
CORES = 2
VMEM_PLAN = 40 * 2**20
VMEM_LIMIT = 60 * 2**20


def line_kernel(
    n_gr, n_fs, n_tp, parts,
    p_ref, gt_ref, ut_ref, dn_ref, sg_ref, su_ref, sd_ref, gain_ref, ids_ref, rw_ref,
    gate_hbm, up_hbm, down_hbm, sg_hbm, su_hbm, sd_hbm, mixed_out,
    x_all, t_all, e_in, w_all, s_in, s_all, q_all, gate_out, up_out, act, part, ru, rd,
    xr, tr, er, sr, fr, qr, ur, dr,
    zs, zd, xs, ys, xd, yd, fs_, ws, ss, sx, qs, us, ds_, loc, res_sem,
):
    gr, z, tp = lax.axis_index("gr"), lax.axis_index("fs"), lax.axis_index("tp")
    y, c = tp // CORES, tp % CORES
    sides = n_tp // CORES
    x_peer, y_other, c_other = 1 - gr, 1 - y, 1 - c
    _, hid, cols = s_in.shape
    sub, width = x_all.shape[2], x_all.shape[3]
    rows = parts * sub
    full = n_gr * n_fs
    quarter = hid // n_fs

    def dev(g, f, t):
        return {"gr": g, "fs": f, "tp": t}

    to_x, to_y = dev(x_peer, z, tp), dev(gr, z, y_other * CORES + c)
    to_c = dev(gr, z, y * CORES + c_other)
    up, down = dev(gr, z + 1, tp), dev(gr, z - 1, tp)
    has_up, has_down = z < n_fs - 1, z > 0

    barrier = pltpu.get_barrier_semaphore()

    def greet(where):
        pl.semaphore_signal(barrier, inc=1, device_id=where, device_id_type=MESH)

    for dz in range(n_fs):
        for dc in range(CORES):
            if dz or dc:
                greet(dev(gr, (z + dz) % n_fs, y * CORES + (c + dc) % CORES))
    greet(to_x)
    greet(to_y)

    gain = gain_ref[...]
    s_in[0] = (sg_ref[...] * gain).astype(jnp.bfloat16)
    s_in[1] = (su_ref[...] * gain).astype(jnp.bfloat16)
    s_in[2] = sd_ref[...].astype(jnp.bfloat16)

    def cast(i, carry):
        f, t = i // n_tp, i % n_tp
        e_in[f, t % CORES, t // CORES, 0] = (gt_ref[i] * gain).astype(jnp.bfloat16)
        e_in[f, t % CORES, t // CORES, 1] = (ut_ref[i] * gain).astype(jnp.bfloat16)
        e_in[f, t % CORES, t // CORES, 2] = dn_ref[i].astype(jnp.bfloat16)
        return carry

    lax.fori_loop(0, n_fs * n_tp, cast, 0)
    for h in range(parts):
        v = p_ref[h * sub : (h + 1) * sub, :].astype(jnp.float32)
        mean = jnp.mean(v * v, axis=-1, keepdims=True)
        x_all[z, h] = (v * lax.rsqrt(mean + eps_norm)).astype(jnp.bfloat16)
    shape = t_all.shape[1:]
    table = jnp.zeros(shape, jnp.float32)
    which = lax.broadcasted_iota(jnp.int32, shape, 0)
    for k in range(ids_ref.shape[0]):
        table = table + jnp.where(ids_ref[k : k + 1, :] == which, rw_ref[k : k + 1, :], 0.0)
    t_all[z] = table
    pl.semaphore_wait(barrier, n_fs * CORES + 1)

    def remote(src, dst, send, recv, where):
        return pltpu.make_async_remote_copy(
            src_ref=src, dst_ref=dst, send_sem=send, recv_sem=recv,
            device_id=where, device_id_type=MESH,
        )

    pending = []

    def go(cond, copies):
        pending.append((cond, copies))

        def start():
            for one in copies:
                one.start()

        if cond is None:
            start()
        else:
            pl.when(cond)(start)

    def slab(g, f, t, core):
        at = pl.ds(pl.multiple_of(t * hid, hid), hid)
        return w_all.at[g * n_fs + f, core, :, :, at, :]

    def got(g, f, t):
        return er.at[(g * n_fs + f) * n_tp + t]

    def send_expert(way, d):
        f = z + d if way == 0 else z - d
        there = f < n_fs if way == 0 else f >= 0
        for i in range(CORES):
            core = c if i == 0 else c_other
            go(there, [remote(
                e_in.at[f, core], slab(gr, z, tp, core), zs.at[way, d, i],
                got(gr, z, tp), dev(gr, f, y * CORES + core),
            )])

    def wait_slab(g, f, t):
        remote(e_in.at[0, 0], slab(g, f, t, c), zs.at[0, 0, 0], got(g, f, t), to_x).wait_recv()

    def pass_slab(g, f, t, sem, where, src=None):
        place = slab(g, f, t, c)
        return remote(place if src is None else src, place, sem, got(g, f, t), where)

    def row_copies(f, h, sem, where):
        copies = [remote(x_all.at[f, h], x_all.at[f, h], sem.at[h], xr.at[f, h], where)]
        if h == 0:
            copies.append(remote(t_all.at[f], t_all.at[f], sem.at[parts], tr.at[f], where))
        return copies

    def s_cols(g, f):
        return s_all.at[:, :, pl.ds(pl.multiple_of((g * n_fs + f) * cols, 128), cols)]

    def s_copy(src, g, f, sem, where):
        return remote(src, s_cols(g, f), sem, sr.at[g * n_fs + f], where)

    mine = e_in.at[z, c]
    own_k = gr * n_fs + z
    locals_ = [
        pltpu.make_async_copy(mine, slab(gr, z, tp, c), loc.at[0]),
        pltpu.make_async_copy(s_in, s_cols(gr, z), loc.at[1]),
    ]
    go(None, [remote(
        e_in.at[z, c_other], slab(gr, z, tp, c_other), zs.at[0, 0, 1], got(gr, z, tp), to_c
    )])
    go(None, [pass_slab(gr, z, tp, xs.at[z * CORES + c], to_x, mine)])
    go(None, [pass_slab(gr, z, tp, ys.at[z * CORES + c], to_y, mine)])
    send_expert(0, 1)
    send_expert(1, 1)
    for one in locals_:
        one.start()
    for h in range(parts):
        go(has_up, row_copies(z, h, zd.at[0, 0], up))
        go(has_down, row_copies(z, h, zd.at[1, 0], down))
    for d in range(2, n_fs):
        send_expert(0, d)
        send_expert(1, d)
    go(has_up, [s_copy(s_in, gr, z, ss.at[0, 0], up)])
    go(has_down, [s_copy(s_in, gr, z, ss.at[1, 0], down)])

    def reach(d):
        if d == 0:
            return [(0, z, None)]
        return [(0, z - d, z - d >= 0), (1, z + d, z + d < n_fs)]

    def when(cond, f):
        if cond is None:
            f()
        else:
            pl.when(cond)(f)

    def own_column(d):
        for _, f, there in reach(d):
            for i in range(CORES):
                if d == 0 and i == 0:
                    continue
                core = c if i == 0 else c_other
                t = y * CORES + core
                when(there, functools.partial(wait_slab, gr, f, t))
                go(there, [
                    pass_slab(gr, f, t, xs.at[f * CORES + core], to_x),
                    pass_slab(gr, f, t, ys.at[f * CORES + core], to_y),
                ])

    def give(g, f, there):
        k = g * n_fs + f
        go(there, [remote(w_all.at[k, c], w_all.at[k, c], fs_.at[k], fr.at[k], to_c)])

        def turn():
            at = pl.ds(pl.multiple_of(k * cols, 128), cols)
            gate_out[at, :] = w_all[k, c, y, 0].T
            up_out[at, :] = w_all[k, c, y, 1].T
            pltpu.make_async_copy(gate_out.at[at, :], gate_hbm.at[at, :], res_sem.at[0, k]).start()
            pltpu.make_async_copy(up_out.at[at, :], up_hbm.at[at, :], res_sem.at[1, k]).start()
            pltpu.make_async_copy(
                w_all.at[k, c, y, 2], down_hbm.at[:, at], res_sem.at[2, k]
            ).start()

        when(there, turn)

    def neighbours(d):
        for _, f, there in reach(d):
            for core in range(CORES):
                when(there, functools.partial(wait_slab, x_peer, f, y * CORES + core))
                if core == 0:
                    go(there, [pass_slab(x_peer, f, y * CORES, yd.at[f], to_y)])
                when(there, functools.partial(wait_slab, gr, f, y_other * CORES + core))
                if core == 1:
                    go(there, [pass_slab(gr, f, y_other * CORES + 1, xd.at[f], to_x)])
            if d == 0:
                locals_[0].wait()
            give(gr, f, there)

    def corners(d):
        for _, f, there in reach(d):
            for core in range(CORES):
                when(there, functools.partial(wait_slab, x_peer, f, y_other * CORES + core))
            give(x_peer, f, there)

    def line_rows(d):
        for h in range(parts):
            for way, f, there in reach(d):
                more = has_up if way == 0 else has_down
                onward = up if way == 0 else down

                def wait(f=f, h=h):
                    for one in row_copies(f, h, zd.at[0, 0], up):
                        one.wait_recv()

                when(there, wait)
                go(there & more, row_copies(f, h, zd.at[way, d], onward))

    def wait_shared(g, f):
        s_copy(s_in, g, f, sx.at[0], to_x).wait_recv()

    def line_shared(d):
        for way, f, there in reach(d):
            more = has_up if way == 0 else has_down
            onward = up if way == 0 else down
            if d:
                when(there, functools.partial(wait_shared, gr, f))
                go(there & more, [s_copy(s_cols(gr, f), gr, f, ss.at[way, d], onward)])
            go(there, [s_copy(s_in if d == 0 else s_cols(gr, f), gr, f, sx.at[f], to_x)])

    own_column(0)
    own_column(1)
    line_shared(0)
    neighbours(0)
    line_rows(1)
    line_shared(1)
    own_column(2)
    neighbours(1)
    line_rows(2)
    line_shared(2)
    own_column(3)
    neighbours(2)
    corners(0)
    line_rows(3)
    line_shared(3)
    locals_[1].wait()
    for f in range(n_fs):
        wait_shared(x_peer, f)

    piece = pl.ds(pl.multiple_of(z * quarter, quarter), quarter)

    def q_at(t):
        return q_all.at[:, pl.ds(pl.multiple_of(t * quarter, quarter), quarter), :]

    def q_copy(src, t, i, where):
        return remote(src, q_at(t), qs.at[i], qr.at[t], where)

    go(None, [q_copy(s_all.at[:, piece, :], tp, 0, to_y)])
    go(None, [q_copy(s_all.at[:, piece, :], tp, 1, to_c)])
    near_q = pltpu.make_async_copy(s_all.at[:, piece, :], q_at(tp), loc.at[2])
    near_q.start()
    t_y = y_other * CORES + c
    q_copy(q_at(t_y), t_y, 2, to_c).wait_recv()
    go(None, [q_copy(q_at(t_y), t_y, 2, to_c)])
    results = [
        pltpu.make_async_copy(s_all.at[i], dst, res_sem.at[3, i])
        for i, dst in enumerate((sg_hbm, su_hbm, sd_hbm))
    ]
    for one in results:
        one.start()
    neighbours(3)
    for d in range(1, n_fs):
        corners(d)
    near_q.wait()
    for side in range(sides):
        t = side * CORES + c_other
        q_copy(q_at(t), t, 2, to_c).wait_recv()
    for k in range(full):
        remote(w_all.at[k, c], w_all.at[k, c_other], fs_.at[k], fr.at[k], to_c).wait_recv()

    def wide(v):
        return v.astype(jnp.float32)

    def nt(a, b):
        return lax.dot_general(a, b, (((1,), (1,)), ((), ())), preferred_element_type=jnp.float32)

    def u_copy(t, h):
        return remote(part.at[t, h], ru.at[t, h], us.at[t, h], ur.at[t, h], up)

    def d_copy(t, h):
        return remote(part.at[t, h], rd.at[t, h], ds_.at[t, h], dr.at[t, h], down)

    def block(p, carry):
        falling = n_fs - 1 - p
        falling = jnp.where(falling <= z, falling - 1, falling)
        rising = jnp.where(p >= z, p + 1, p)
        t = jnp.where(p == n_fs - 1, z, jnp.where(z < n_fs // 2, falling, rising))
        xs_t = x_all[t].reshape(rows, width)
        both = nt(xs_t, q_all[0:2].reshape(2 * hid, width))
        extra = (jax.nn.silu(both[:, :hid]) * both[:, hid:]).astype(jnp.bfloat16)

        def expert(s, inner):
            core, side = s // sides, s % sides
            total = None
            for k in range(full):
                w = w_all[k, core, side, 0:2].reshape(2 * n_tp * hid, cols)
                one = nt(xs_t[:, k * cols : (k + 1) * cols], w)
                total = one if total is None else total + one
            e = z * n_tp + side * CORES + core
            scale = jnp.broadcast_to(t_all[t, pl.ds(e, 1), :], (rows, rows)).T[:, :1]
            val = jax.nn.silu(total[:, : n_tp * hid]) * total[:, n_tp * hid :] * scale
            act[s] = val.astype(jnp.bfloat16)
            return inner

        lax.fori_loop(0, n_tp, expert, 0)

        def columns(k, inner):
            at = pl.ds(pl.multiple_of(k * cols, 128), cols)
            total = jnp.dot(extra, q_all[2, :, at], preferred_element_type=jnp.float32)
            for s in range(n_tp):
                total = total + jnp.dot(
                    act[s], w_all[k, s // sides, s % sides, 2], preferred_element_type=jnp.float32
                )
            part[t, :, :, at] = total.astype(jnp.bfloat16).reshape(parts, sub, cols)
            return inner

        lax.fori_loop(0, full, columns, 0)
        for h in range(parts):
            pl.when((t > z) & jnp.logical_not(has_down))(lambda: u_copy(t, h).start())
            pl.when((t < z) & jnp.logical_not(has_up))(lambda: d_copy(t, h).start())
        return carry

    lax.fori_loop(0, n_fs, block, 0)

    for d in range(n_fs - 1, 0, -1):
        for h in range(parts):
            for way, there, before in (
                (0, z + d < n_fs, has_down),
                (1, z - d >= 0, has_up),
            ):
                t = z + d if way == 0 else z - d
                copy, arrived = (u_copy, ru) if way == 0 else (d_copy, rd)

                @pl.when(there & before)
                def _(t=t, h=h, copy=copy, arrived=arrived):
                    copy(t, h).wait_recv()
                    part[t, h] = (wide(part[t, h]) + wide(arrived[t, h])).astype(jnp.bfloat16)
                    copy(t, h).start()

    for h in range(parts):

        @pl.when(has_down & has_up)
        def _(h=h):
            u_copy(z, h).wait_recv()
            d_copy(z, h).wait_recv()
            mixed_out[h] = (
                wide(part[z, h]) + wide(ru[z, h]) + wide(rd[z, h])
            ).astype(jnp.bfloat16)

        @pl.when(jnp.logical_not(has_up))
        def _(h=h):
            u_copy(z, h).wait_recv()
            mixed_out[h] = (wide(part[z, h]) + wide(ru[z, h])).astype(jnp.bfloat16)

        @pl.when(jnp.logical_not(has_down))
        def _(h=h):
            d_copy(z, h).wait_recv()
            mixed_out[h] = (wide(part[z, h]) + wide(rd[z, h])).astype(jnp.bfloat16)

    for one in results:
        one.wait()
    for k in range(full):
        at = pl.ds(k * cols, cols)
        pltpu.make_async_copy(gate_out.at[at, :], gate_hbm.at[at, :], res_sem.at[0, k]).wait()
        pltpu.make_async_copy(up_out.at[at, :], up_hbm.at[at, :], res_sem.at[1, k]).wait()
        pltpu.make_async_copy(w_all.at[k, c, y, 2], down_hbm.at[:, at], res_sem.at[2, k]).wait()
    for cond, copies in pending:
        when(cond, lambda copies=copies: [one.wait_send() for one in copies] and None)
    for d in range(1, n_fs):
        for h in range(parts):
            pl.when(z + d < n_fs)(lambda d=d, h=h: u_copy(z + d, h).wait_send())
            pl.when(z - d >= 0)(lambda d=d, h=h: d_copy(z - d, h).wait_send())


def copy_kernel(count, *refs):
    ins, outs, bufs, sems = refs[:count], refs[count : 2 * count], refs[2 * count : -1], refs[-1]
    loads = [pltpu.make_async_copy(ins[i], bufs[i], sems.at[0, i]) for i in range(count)]
    stores = [pltpu.make_async_copy(bufs[i], outs[i], sems.at[1, i]) for i in range(count)]
    for one in loads:
        one.start()
    for one, then in zip(loads, stores):
        one.wait()
        then.start()
    for one in stores:
        one.wait()


def copied(arrays):
    count = len(arrays)
    return pl.pallas_call(
        functools.partial(copy_kernel, count),
        out_shape=tuple(jax.ShapeDtypeStruct(a.shape, a.dtype) for a in arrays),
        in_specs=[pl.BlockSpec(memory_space=pl.ANY)] * count,
        out_specs=(pl.BlockSpec(memory_space=pl.ANY),) * count,
        scratch_shapes=[pltpu.VMEM(a.shape, a.dtype) for a in arrays]
        + [pltpu.SemaphoreType.DMA((2, count))],
        compiler_params=pltpu.CompilerParams(vmem_limit_bytes=VMEM_LIMIT),
    )(*arrays)


def line_body(
    n_gr, n_fs, n_tp,
    prompt, train_gate, train_up, train_down, train_shared_gate, train_shared_up,
    train_shared_down, norm_gain, expert_ids, route_weight,
):
    experts, cols, hid = train_gate.shape
    rows, width = prompt.shape
    full, parts, sides = n_gr * n_fs, 2, n_tp // CORES
    sub, wide_hid = rows // parts, n_tp * hid
    bf16 = jnp.bfloat16
    vmem = pl.BlockSpec(memory_space=pltpu.VMEM)
    dma = pltpu.SemaphoreType.DMA
    shape = jax.ShapeDtypeStruct
    outs = pl.pallas_call(
        functools.partial(line_kernel, n_gr, n_fs, n_tp, parts),
        out_shape=(
            shape((width, wide_hid), bf16),
            shape((width, wide_hid), bf16),
            shape((wide_hid, width), bf16),
            shape((hid, width), bf16),
            shape((hid, width), bf16),
            shape((hid, width), bf16),
            shape((parts, sub, width), bf16),
        ),
        in_specs=[vmem] * 10,
        out_specs=(pl.BlockSpec(memory_space=pl.ANY),) * 6 + (vmem,),
        scratch_shapes=[
            pltpu.VMEM((n_fs, parts, sub, width), bf16),
            pltpu.VMEM((n_fs, experts, rows), jnp.float32),
            pltpu.VMEM((n_fs, CORES, sides, 3, hid, cols), bf16),
            pltpu.VMEM((full, CORES, sides, 3, wide_hid, cols), bf16),
            pltpu.VMEM((3, hid, cols), bf16),
            pltpu.VMEM((3, hid, width), bf16),
            pltpu.VMEM((3, hid, width), bf16),
            pltpu.VMEM((width, wide_hid), bf16),
            pltpu.VMEM((width, wide_hid), bf16),
            pltpu.VMEM((n_tp, rows, wide_hid), bf16),
            pltpu.VMEM((n_fs, parts, sub, width), bf16),
            pltpu.VMEM((n_fs, parts, sub, width), bf16),
            pltpu.VMEM((n_fs, parts, sub, width), bf16),
            dma((n_fs, parts)), dma((n_fs,)), dma((full * n_tp,)), dma((full,)), dma((full,)),
            dma((n_tp,)), dma((n_fs, parts)), dma((n_fs, parts)),
            dma((2, n_fs, CORES)), dma((2, n_fs, parts + 1)), dma((n_fs * CORES,)),
            dma((n_fs * CORES,)), dma((n_fs,)), dma((n_fs,)), dma((full,)), dma((1,)),
            dma((2, n_fs)), dma((n_fs,)), dma((3,)), dma((n_fs, parts)), dma((n_fs, parts)),
            dma((3,)), dma((4, full)),
        ],
        compiler_params=pltpu.CompilerParams(
            collective_id=0, has_side_effects=True, vmem_limit_bytes=VMEM_LIMIT
        ),
    )(
        prompt, train_gate.transpose(0, 2, 1), train_up.transpose(0, 2, 1), train_down,
        train_shared_gate.T, train_shared_up.T, train_shared_down, norm_gain[None, :],
        expert_ids.T, route_weight.T,
    )
    serve_gate, serve_up, serve_down, s_gate, s_up, s_down, mixed_out = copied(outs)
    return (
        serve_gate[None], serve_up[None], serve_down[None],
        s_gate.T, s_up.T, s_down, mixed_out.reshape(rows, width),
    )


def regroup(stacked, lowered):
    stacked = lax.all_to_all(
        lax.all_to_all(stacked, "fs", split_axis=0, concat_axis=2, tiled=True),
        "tp",
        split_axis=0,
        concat_axis=3,
        tiled=True,
    )
    lowered = lax.all_to_all(
        lax.all_to_all(lowered, "fs", split_axis=0, concat_axis=2, tiled=True),
        "tp",
        split_axis=0,
        concat_axis=1,
        tiled=True,
    )
    return (stacked, lowered)


def body(
    prompt,
    train_gate,
    train_up,
    train_down,
    train_shared_gate,
    train_shared_up,
    train_shared_down,
    norm_gain,
    expert_ids,
    route_weight,
):
    gain_col = norm_gain[:, None]
    stacked = jnp.stack((train_gate * gain_col[None], train_up * gain_col[None]), axis=1).astype(
        jnp.bfloat16
    )
    lowered = train_down.astype(jnp.bfloat16)
    stacked, lowered = regroup(stacked, lowered)
    stacked, lowered = (
        lax.all_gather(stacked, "gr", axis=2, tiled=True),
        lax.all_gather(lowered, "gr", axis=2, tiled=True),
    )
    serve_gate = stacked[:, 0]
    serve_up = stacked[:, 1]
    serve_shared_gate, serve_shared_up, serve_shared_down = (
        lax.all_gather(
            (train_shared_gate * gain_col).astype(jnp.bfloat16), ("gr", "fs"), axis=0, tiled=True
        ),
        lax.all_gather(
            (train_shared_up * gain_col).astype(jnp.bfloat16), ("gr", "fs"), axis=0, tiled=True
        ),
        lax.all_gather(train_shared_down.astype(jnp.bfloat16), ("gr", "fs"), axis=1, tiled=True),
    )
    widened = prompt.astype(jnp.float32)
    normed = (
        widened * lax.rsqrt(jnp.mean(widened * widened, axis=-1, keepdims=True) + eps_norm)
    ).astype(jnp.bfloat16)
    block_rows = lax.all_gather(normed, "tp", axis=0, tiled=True)
    gate_val = jnp.dot(block_rows, serve_shared_gate, preferred_element_type=jnp.float32)
    up_val = jnp.dot(block_rows, serve_shared_up, preferred_element_type=jnp.float32)
    shared_act = (jax.nn.silu(gate_val) * up_val).astype(jnp.bfloat16)
    shared_sum = lax.psum_scatter(
        jnp.dot(shared_act, serve_shared_down, preferred_element_type=jnp.float32).astype(
            jnp.bfloat16
        ),
        "tp",
        scatter_dimension=0,
        tiled=True,
    ).astype(jnp.float32)
    row_count = prompt.shape[0]
    top_count = expert_ids.shape[1]
    model_width = prompt.shape[1]
    expert_count = lax.axis_size("fs") * lax.axis_size("tp")
    capacity = row_count * top_count // expert_count + 1
    flat_ids = expert_ids.reshape(-1)
    onehot = (flat_ids[:, None] == jnp.arange(expert_count, dtype=jnp.int32)[None, :]).astype(
        jnp.int32
    )
    earlier = jnp.cumsum(onehot, axis=0) - onehot
    places = jnp.sum(earlier * onehot, axis=1)
    slot_ids = (flat_ids * capacity + places).reshape(row_count, top_count)
    slot_range = jnp.arange(expert_count * capacity, dtype=jnp.int32)
    dispatch = jnp.any(slot_range[:, None, None] == slot_ids[None, :, :], axis=-1).astype(
        jnp.bfloat16
    )
    outgoing = jnp.dot(dispatch, normed, preferred_element_type=jnp.float32).astype(jnp.bfloat16)
    outgoing = outgoing.reshape(expert_count, capacity, model_width)
    arrived = lax.all_to_all(outgoing, ("fs", "tp"), split_axis=0, concat_axis=0, tiled=True)
    source_count, slot_count, width_here = arrived.shape
    arrived_rows = arrived.reshape(source_count * slot_count, width_here)
    gate_val = jnp.dot(arrived_rows, serve_gate[0], preferred_element_type=jnp.float32)
    up_val = jnp.dot(arrived_rows, serve_up[0], preferred_element_type=jnp.float32)
    hidden = (jax.nn.silu(gate_val) * up_val).astype(jnp.bfloat16)
    result = jnp.dot(hidden, lowered[0], preferred_element_type=jnp.float32).astype(jnp.bfloat16)
    result = result.reshape(source_count, slot_count, width_here)
    returned = lax.all_to_all(result, ("fs", "tp"), split_axis=0, concat_axis=0, tiled=True)
    picked = returned.reshape(expert_count * capacity, model_width)[slot_ids]
    routed = jnp.sum(route_weight[:, :, None] * picked.astype(jnp.float32), axis=1)
    mixed_out = (routed + shared_sum).astype(jnp.bfloat16)
    return (
        serve_gate,
        serve_up,
        lowered,
        serve_shared_gate,
        serve_shared_up,
        serve_shared_down,
        mixed_out,
    )


def solution(mesh):
    placed = (
        P(("gr", "fs", "tp"), None),
        P(None, ("gr", "fs"), "tp"),
        P(None, ("gr", "fs"), "tp"),
        P(None, "tp", ("gr", "fs")),
        P(("gr", "fs"), "tp"),
        P(("gr", "fs"), "tp"),
        P("tp", ("gr", "fs")),
        P(("gr", "fs")),
        P(("gr", "fs", "tp"), None),
        P(("gr", "fs", "tp"), None),
    )
    n_gr, n_fs, n_tp = (mesh.shape[name] for name in ("gr", "fs", "tp"))

    def chosen(prompt, train_gate, *rest):
        rows, width = prompt.shape
        experts, cols, hid = train_gate.shape
        held = n_fs * n_tp * n_gr * CORES * 3 * hid * cols * 4 + 4 * n_fs * prompt.size * 2
        fits = n_gr == 2 and n_tp == 2 * CORES and n_fs % 2 == 0 and held < VMEM_PLAN
        even = experts == n_fs * n_tp and cols * n_gr * n_fs == width and rows == 128
        if fits and even and hid % (16 * n_fs) == 0 and cols % 128 == 0:
            return line_body(n_gr, n_fs, n_tp, prompt, train_gate, *rest)
        return body(prompt, train_gate, *rest)

    return jax.shard_map(
        chosen,
        mesh=mesh,
        in_specs=placed,
        out_specs=(
            P(("fs", "tp"), None, None),
            P(("fs", "tp"), None, None),
            P(("fs", "tp"), None, None),
            P(None, "tp"),
            P(None, "tp"),
            P("tp", None),
            P(("gr", "fs", "tp"), None),
        ),
        check_vma=False,
    )
```

time: 164 us -> 141 us (0.86)
  the two profiles are of different devices: /device:TPU:24 before, /device:TPU:0 now
where the time goes in v1:
time: 141 us; the launch traced here: 140 us
  Pallas kernels  140 us (99%)
    pallas_call x1, Pallas kernels, line_body(): pl.pallas_call(functools.partial(line_kernel, n_gr, n_fs, n_tp, parts), o...  136 us
    pallas_call x1, Pallas kernels, copied(): pl.pallas_call(functools.partial(copy_kernel, count), out_shape=tuple((ja...  3.44 us

profile of v1, /device:TPU:0, one launch (start us, length us, event | category | flops | bytes accessed | tf_op | source)
XLA Modules:
  0.0 140.3 jit_solution(10841074825911486281)
XLA Ops:
  0.6 136.2 %shard_map.153 = (bf16[2048,256]{1,0:T(8,128)(2,1)}, bf16[2048,256]{1,0:T(8,128)(2,1)}, bf16[256,2048]{1,0:T(8,128)(2,1)}, bf16[64,2048]{1,0:T(8,128)(2,1)}, bf1...) custom-call(bf16[128,2048]{1,0:T(8,128)(2,1)} %p_ref.1, f32[16,64,256]{2,1,0:T(8,128)} %bitcast.13, ...), custom_call_target="tpu_custom_call" | custom-call | tf_op jit(solution)/shard_map/pallas_call | solution.py:437
  136.8 3.4 %shard_map.154 = (bf16[2048,256]{1,0:T(8,128)(2,1)}, bf16[2048,256]{1,0:T(8,128)(2,1)}, bf16[256,2048]{1,0:T(8,128)(2,1)}, bf16[64,2048]{1,0:T(8,128)(2,1)}, bf1...) custom-call(bf16[2048,256]{1,0:T(8,128)(2,1)} %get-tuple-element.21.refs_0_, ...), custom_call_target="tpu_custom_call" | custom-call | tf_op jit(solution)/shard_map/pallas_call | solution.py:413

commit v2 on v1

v2 whole, which is shorter than its diff:
```python
import functools

import jax
import jax.numpy as jnp
from jax import lax
from jax.experimental import pallas as pl
from jax.experimental.pallas import tpu as pltpu
from jax.sharding import PartitionSpec as P

eps_norm = 1e-06
MESH = pl.DeviceIdType.MESH
CORES = 2
VMEM_PLAN = 40 * 2**20
VMEM_LIMIT = 60 * 2**20


def line_kernel(
    n_gr, n_fs, n_tp, parts,
    p_hbm, gt_hbm, ut_hbm, dn_hbm, tsg_hbm, tsu_hbm, tsd_hbm, gain_hbm, ids_hbm, rw_hbm,
    gate_hbm, up_hbm, down_hbm, sg_hbm, su_hbm, sd_hbm, mixed_hbm,
    p_ref, gt_ref, ut_ref, dn_ref, sg_ref, su_ref, sd_ref, gain_ref, ids_ref, rw_ref,
    x_all, t_all, e_in, w_all, s_in, s_all, gate_out, up_out, acc, act, base, mixed_out,
    part, ru, rd,
    xr, tr, er, sr, sc, fr, ur, dr,
    zs, zd, xs, ys, xd, yd, fs_, ss, sx, sy, sd, us, ds_, loc, res_sem, in_sem,
):
    gr, z, tp = lax.axis_index("gr"), lax.axis_index("fs"), lax.axis_index("tp")
    y, c = tp // CORES, tp % CORES
    sides = n_tp // CORES
    x_peer, y_other, c_other = 1 - gr, 1 - y, 1 - c
    _, hid, cols = s_in.shape
    sub, width = x_all.shape[2], x_all.shape[3]
    rows = parts * sub
    full = n_gr * n_fs
    wide_hid = n_tp * hid

    def dev(g, f, t):
        return {"gr": g, "fs": f, "tp": t}

    to_x, to_y = dev(x_peer, z, tp), dev(gr, z, y_other * CORES + c)
    to_c = dev(gr, z, y * CORES + c_other)
    up, down = dev(gr, z + 1, tp), dev(gr, z - 1, tp)
    has_up, has_down = z < n_fs - 1, z > 0
    inner = has_up & has_down
    outer = jnp.logical_not(inner)

    def far(p):
        if p == n_fs - 1:
            return z
        fall, rise = n_fs - 1 - p, p
        fall = jnp.where(fall <= z, fall - 1, fall)
        rise = jnp.where(rise >= z, rise + 1, rise)
        return jnp.where(z < n_fs // 2, fall, rise)

    order = [far(n_fs - 1 - p) for p in range(n_fs)]

    def place(f, at):
        rise = jnp.where(f < at, f + 1, f)
        fall = jnp.where(f > at, n_fs - f, n_fs - 1 - f)
        return jnp.where(f == at, 0, jnp.where(at < n_fs // 2, rise, fall))

    ins = [
        pltpu.make_async_copy(src, dst, in_sem.at[i])
        for i, (src, dst) in enumerate((
            (gain_hbm, gain_ref), (gt_hbm, gt_ref), (ut_hbm, ut_ref), (dn_hbm, dn_ref),
            (tsg_hbm, sg_ref), (tsu_hbm, su_ref), (tsd_hbm, sd_ref), (p_hbm, p_ref),
            (ids_hbm, ids_ref), (rw_hbm, rw_ref),
        ))
    ]
    for one in ins:
        one.start()

    barrier = pltpu.get_barrier_semaphore()

    def greet(where):
        pl.semaphore_signal(barrier, inc=1, device_id=where, device_id_type=MESH)

    for dz in range(n_fs):
        for dc in range(CORES):
            if dz or dc:
                greet(dev(gr, (z + dz) % n_fs, y * CORES + (c + dc) % CORES))
    greet(to_x)
    greet(to_y)

    for one in ins[:4]:
        one.wait()
    gain = gain_ref[...]

    def cast(i, carry):
        f, t = i // n_tp, i % n_tp
        e_in[f, t % CORES, t // CORES, 0] = (gt_ref[i] * gain).astype(jnp.bfloat16)
        e_in[f, t % CORES, t // CORES, 1] = (ut_ref[i] * gain).astype(jnp.bfloat16)
        e_in[f, t % CORES, t // CORES, 2] = dn_ref[i].astype(jnp.bfloat16)
        return carry

    lax.fori_loop(0, n_fs * n_tp, cast, 0)
    pl.semaphore_wait(barrier, n_fs * CORES + 1)

    def remote(src, dst, send, recv, where):
        return pltpu.make_async_remote_copy(
            src_ref=src, dst_ref=dst, send_sem=send, recv_sem=recv,
            device_id=where, device_id_type=MESH,
        )

    pending = []

    def when(cond, f):
        if cond is None:
            f()
        else:
            pl.when(cond)(f)

    def go(cond, copies):
        pending.append((cond, copies))

        def start():
            for one in copies:
                one.start()

        when(cond, start)

    def slab(g, f, t, core):
        at = pl.ds(pl.multiple_of(t * hid, hid), hid)
        return w_all.at[g * n_fs + f, core, :, :, at, :]

    def got(g, f, t):
        return er.at[(g * n_fs + f) * n_tp + t]

    def send_expert(d, i):
        core = c if i == 0 else c_other
        for way in (0, 1):
            f = z + d if way == 0 else z - d
            there = f < n_fs if way == 0 else f >= 0
            go(there, [remote(
                e_in.at[f, core], slab(gr, z, tp, core), zs.at[way, d, i],
                got(gr, z, tp), dev(gr, f, y * CORES + core),
            )])

    def wait_slab(g, f, t):
        remote(e_in.at[0, 0], slab(g, f, t, c), zs.at[0, 0, 0], got(g, f, t), to_x).wait_recv()

    def pass_slab(g, f, t, sem, where, src=None):
        place = slab(g, f, t, c)
        return remote(place if src is None else src, place, sem, got(g, f, t), where)

    def row_copies(f, h, sem, way):
        to = z + 1 if way == 0 else z - 1
        here, there = place(f, z), place(f, to)
        where = dev(gr, to, tp)
        copies = [remote(x_all.at[here, h], x_all.at[there, h], sem.at[h], xr.at[f, h], where)]
        if h == 0:
            copies.append(remote(t_all.at[f], t_all.at[f], sem.at[parts], tr.at[f], where))
        return copies

    def s_slab(g, f, t):
        lanes = pl.ds(pl.multiple_of((g * n_fs + f) * cols, 128), cols)
        return s_all.at[:, pl.ds(pl.multiple_of(t * hid, hid), hid), lanes]

    def s_copy(src, g, f, sem, where, t=tp):
        src = s_slab(g, f, t) if src is None else src
        return remote(src, s_slab(g, f, t), sem, sr.at[(g * n_fs + f) * n_tp + t], where)

    mine = e_in.at[z, c]
    go(None, [remote(
        e_in.at[z, c_other], slab(gr, z, tp, c_other), zs.at[0, 0, 1], got(gr, z, tp), to_c
    )])
    go(None, [pass_slab(gr, z, tp, xs.at[z * CORES + c], to_x, mine)])
    go(None, [pass_slab(gr, z, tp, ys.at[z * CORES + c], to_y, mine)])
    for i in range(CORES):
        for d in range(1, n_fs):
            send_expert(d, i)
    near_slab = pltpu.make_async_copy(mine, slab(gr, z, tp, c), loc.at[0])
    near_slab.start()

    for one in ins[4:]:
        one.wait()
    s_in[0] = (sg_ref[...] * gain).astype(jnp.bfloat16)
    s_in[1] = (su_ref[...] * gain).astype(jnp.bfloat16)
    s_in[2] = sd_ref[...].astype(jnp.bfloat16)
    for h in range(parts):
        v = p_ref[h * sub : (h + 1) * sub, :].astype(jnp.float32)
        mean = jnp.mean(v * v, axis=-1, keepdims=True)
        x_all[0, h] = (v * lax.rsqrt(mean + eps_norm)).astype(jnp.bfloat16)
    shape = t_all.shape[1:]
    table = jnp.zeros(shape, jnp.float32)
    which = lax.broadcasted_iota(jnp.int32, shape, 0)
    for k in range(ids_ref.shape[0]):
        table = table + jnp.where(ids_ref[k : k + 1, :] == which, rw_ref[k : k + 1, :], 0.0)
    t_all[z] = table

    near_s = pltpu.make_async_copy(s_in, s_slab(gr, z, tp), loc.at[1])
    near_s.start()

    def send_own(cond):
        for h in range(parts):
            for way in (0, 1):
                there = has_up if way == 0 else has_down
                go(there & cond, row_copies(z, h, zd.at[way], way))
        go(has_up & cond, [s_copy(s_in, gr, z, ss.at[0], up)])
        go(has_down & cond, [s_copy(s_in, gr, z, ss.at[1], down)])

    send_own(True)

    def own(p, i):
        f = order[p]
        core = c if i == 0 else c_other
        t = y * CORES + core
        wait_slab(gr, f, t)
        go(None, [pass_slab(gr, f, t, xs.at[f * CORES + core], to_x)])
        go(None, [pass_slab(gr, f, t, ys.at[f * CORES + core], to_y)])

    def result_copies(k):
        at = pl.ds(pl.multiple_of(k * cols, 128), cols)
        return [
            pltpu.make_async_copy(gate_out.at[at, :], gate_hbm.at[at, :], res_sem.at[0, k]),
            pltpu.make_async_copy(up_out.at[at, :], up_hbm.at[at, :], res_sem.at[1, k]),
            pltpu.make_async_copy(w_all.at[k, c, y, 2], down_hbm.at[:, at], res_sem.at[2, k]),
        ]

    def give(g, f):
        k = g * n_fs + f
        go(None, [remote(w_all.at[k, c], w_all.at[k, c], fs_.at[k], fr.at[k], to_c)])
        at = pl.ds(pl.multiple_of(k * cols, 128), cols)
        gate_out[at, :] = w_all[k, c, y, 0].T
        up_out[at, :] = w_all[k, c, y, 1].T
        for one in result_copies(k):
            one.start()

    def side(p, core):
        f = order[p]
        wait_slab(x_peer, f, y * CORES + core)
        if core == 0:
            go(None, [pass_slab(x_peer, f, y * CORES, yd.at[f], to_y)])
        wait_slab(gr, f, y_other * CORES + core)
        if core == 1:
            go(None, [pass_slab(gr, f, y_other * CORES + 1, xd.at[f], to_x)])

    def column(p):
        if p == 0:
            near_slab.wait()
        give(gr, order[p])

    def corner(p):
        f = order[p]
        for core in range(CORES):
            wait_slab(x_peer, f, y_other * CORES + core)
        give(x_peer, f)

    def row_part(p, h, most=None):
        f = order[p]

        def arrive():
            remote(x_all.at[p, h], x_all.at[p, h], zd.at[0, 0], xr.at[f, h], to_x).wait_recv()
            if h == 0:
                remote(t_all.at[f], t_all.at[f], zd.at[0, 0], tr.at[f], to_x).wait_recv()

        when(most, arrive)
        if most is inner:
            go((f < z) & inner, row_copies(f, h, zd.at[1 + p], 0))
            go((f > z) & inner, row_copies(f, h, zd.at[n_fs + p], 1))

    def wait_shared(g, f, t):
        s_copy(None, g, f, sx.at[0], to_x, t).wait_recv()

    def shared(p, most=True):
        f = order[p]
        src = None if p else s_in
        if p:
            when(None if most is True else most, functools.partial(wait_shared, gr, f, tp))
            go((f < z) & has_up & most, [s_copy(src, gr, f, ss.at[1 + p], up)])
            go((f > z) & has_down & most, [s_copy(src, gr, f, ss.at[n_fs + p], down)])
        most = None if most is True else most
        go(most, [s_copy(src, gr, f, sx.at[f], to_x)])
        go(most, [s_copy(src, gr, f, sy.at[gr * n_fs + f], to_y)])

    def shared_x(p):
        f = order[p]
        wait_shared(x_peer, f, tp)
        go(None, [s_copy(None, x_peer, f, sy.at[x_peer * n_fs + f], to_y)])

    def nt(a, b):
        return lax.dot_general(a, b, (((1,), (1,)), ((), ())), preferred_element_type=jnp.float32)

    def step(g, f, first=False):
        k = g * n_fs + f
        remote(w_all.at[k, c], w_all.at[k, c_other], fs_.at[k], fr.at[k], to_c).wait_recv()
        at = pl.ds(pl.multiple_of(k * cols, 128), cols)
        some = (n_fs - 1) * rows
        lhs = x_all[0 : n_fs - 1, :, :, at].reshape(some, cols)
        for s in range(n_tp):
            w = w_all[k, s // sides, s % sides, 0:2].reshape(2 * wide_hid, cols)
            val = nt(lhs, w)
            acc[s, 0:some] = val if first else acc[s, 0:some] + val

    def late():
        lhs = x_all[n_fs - 1].reshape(rows, width)

        def one(s, carry):
            total = None
            for k in range(full):
                w = w_all[k, s // sides, s % sides, 0:2].reshape(2 * wide_hid, cols)
                val = nt(lhs[:, k * cols : (k + 1) * cols], w)
                total = val if total is None else total + val
            acc[s, (n_fs - 1) * rows :] = total
            return carry

        lax.fori_loop(0, n_tp, one, 0)

    def s_slice(t):
        return s_all.at[:, pl.ds(pl.multiple_of(t * hid, hid), hid), :]

    def s_whole(t, i):
        return remote(s_slice(t), s_slice(t), sd.at[i], sc.at[t], to_c)

    s_results = [
        pltpu.make_async_copy(s_slice(tp).at[i], dst, res_sem.at[3, i])
        for i, dst in enumerate((sg_hbm, su_hbm, sd_hbm))
    ]
    t_y = y_other * CORES + c

    def shared_give():
        near_s.wait()
        go(None, [s_whole(tp, 0)])
        for one in s_results:
            one.start()
        for g in range(n_gr):
            for f in range(n_fs):
                wait_shared(g, f, t_y)
        go(None, [s_whole(t_y, 1)])

    def shared_act():
        for side in range(sides):
            s_whole(side * CORES + c_other, 0).wait_recv()
        lhs = x_all[0].reshape(rows, width)
        both = nt(lhs, s_all[0:2].reshape(2 * wide_hid, width))
        act[0] = (jax.nn.silu(both[:, :wide_hid]) * both[:, wide_hid:]).astype(jnp.bfloat16)

        def columns(k, inner):
            at = pl.ds(pl.multiple_of(k * cols, 128), cols)
            val = jnp.dot(act[0], s_all[2, :, at], preferred_element_type=jnp.float32)
            base[:, at] = val
            return inner

        lax.fori_loop(0, full, columns, 0)

    stages = []

    def then(f, *args):
        stages.append((f, args))

    def wide(v):
        return v.astype(jnp.float32)

    def u_copy(t, h):
        return remote(part.at[t, h], ru.at[t, h], us.at[t, h], ur.at[t, h], up)

    def d_copy(t, h):
        return remote(part.at[t, h], rd.at[t, h], ds_.at[t, h], dr.at[t, h], down)

    def when_way(t, ahead, behind):
        pl.when(t > z)(ahead)
        pl.when(t < z)(behind)

    def block(p):
        t = order[p]
        here = slice(p * rows, (p + 1) * rows)

        for s in range(n_tp):
            e = z * n_tp + (s % sides) * CORES + s // sides
            scale = jnp.broadcast_to(t_all[t, pl.ds(e, 1), :], (rows, rows)).T[:, :1]
            val = acc[s, here, :]
            val = jax.nn.silu(val[:, :wide_hid]) * val[:, wide_hid:] * scale
            act[s] = val.astype(jnp.bfloat16)

        group = 4

        def columns(j, carry):
            for i in range(group):
                k = j * group + i
                at = pl.ds(pl.multiple_of(k * cols, 128), cols)
                total = None
                for s in range(n_tp):
                    val = jnp.dot(
                        act[s], w_all[k, s // sides, s % sides, 2],
                        preferred_element_type=jnp.float32,
                    )
                    total = val if total is None else total + val
                part[t, :, :, at] = total.astype(jnp.bfloat16).reshape(parts, sub, cols)
            return carry

        lax.fori_loop(0, full // group, columns, 0)
        if p:
            for h in range(parts):
                pl.when((t > z) & jnp.logical_not(has_down))(lambda: u_copy(t, h).start())
                pl.when((t < z) & jnp.logical_not(has_up))(lambda: d_copy(t, h).start())

    def chain(p):
        t = order[p]
        for h in range(parts):
            for copy, arrived, cond in (
                (u_copy, ru, (t > z) & has_down), (d_copy, rd, (t < z) & has_up)
            ):

                @pl.when(cond)
                def _(h=h, copy=copy, arrived=arrived):
                    with jax.named_scope("chain"):
                        copy(t, h).wait_recv()
                    part[t, h] = (wide(part[t, h]) + wide(arrived[t, h])).astype(jnp.bfloat16)
                    copy(t, h).start()

    def mixed_copy(h):
        return pltpu.make_async_copy(mixed_out.at[h], mixed_hbm.at[h], loc.at[2 + h])

    def finish(h):
        mine_h = slice(h * sub, (h + 1) * sub)

        def total(*arrived):
            val = wide(part[z, h]) + base[mine_h, :]
            for one in arrived:
                val = val + wide(one)
            mixed_out[h] = val.astype(jnp.bfloat16)

        @pl.when(has_down & has_up)
        def _():
            u_copy(z, h).wait_recv()
            d_copy(z, h).wait_recv()
            total(ru[z, h], rd[z, h])

        @pl.when(jnp.logical_not(has_up))
        def _():
            u_copy(z, h).wait_recv()
            total(ru[z, h])

        @pl.when(jnp.logical_not(has_down))
        def _():
            d_copy(z, h).wait_recv()
            total(rd[z, h])

        mixed_copy(h).start()

    last = n_fs - 1
    then(own, 0, 1)
    for i in range(CORES):
        for p in range(1, n_fs):
            then(own, p, i)
            if i == 0 and p == last:
                then(side, 0, 0)
                then(side, 0, 1)
                then(column, 0)
    for p in range(1, last):
        then(side, p, 0)
        then(side, p, 1)
        then(column, p)
    for h in range(parts):
        for p in range(1, last):
            then(row_part, p, h, inner)
    then(corner, 0)
    then(side, last, 0)
    then(side, last, 1)
    then(column, last)
    then(shared, 0)
    for p in range(1, last):
        for h in range(parts):
            then(row_part, p, h, outer)
        then(shared, p, inner)
    then(corner, 1)
    for p in range(n_fs):
        then(step, gr, order[p], p == 0)
    for p in range(2):
        then(step, x_peer, order[p])
    then(shared, 1, outer)
    for p in range(2, n_fs):
        then(row_part, last, p - 2, inner)
        then(corner, p)
        then(step, x_peer, order[p])
    then(block, last - 1)
    then(shared, last, inner)
    for h in range(parts):
        then(row_part, last, h, outer)
    then(late)
    then(block, last)
    for p in range(1, last - 1):
        then(block, p)
    for p in range(2, n_fs):
        then(shared, p, outer)
    then(block, 0)
    then(chain, last - 1)
    for p in range(n_fs):
        then(shared_x, p)
    then(chain, last)
    then(shared_give)
    then(shared_act)
    for p in range(1, last - 1):
        then(chain, p)
    for h in range(parts):
        then(finish, h)

    for f, args in stages:
        with jax.named_scope(f.__name__ + "_".join(str(a) for a in args if type(a) is int)):
            f(*args)

    with jax.named_scope("drain"):
        for h in range(parts):
            mixed_copy(h).wait()
        for one in s_results:
            one.wait()
        for k in range(full):
            for one in result_copies(k):
                one.wait()
        for cond, copies in pending:
            when(cond, lambda copies=copies: [one.wait_send() for one in copies] and None)
        for d in range(1, n_fs):
            for h in range(parts):
                pl.when(z + d < n_fs)(lambda d=d, h=h: u_copy(z + d, h).wait_send())
                pl.when(z - d >= 0)(lambda d=d, h=h: d_copy(z - d, h).wait_send())


def copy_kernel(count, *refs):
    ins, outs, bufs, sems = refs[:count], refs[count : 2 * count], refs[2 * count : -1], refs[-1]
    loads = [pltpu.make_async_copy(ins[i], bufs[i], sems.at[0, i]) for i in range(count)]
    stores = [pltpu.make_async_copy(bufs[i], outs[i], sems.at[1, i]) for i in range(count)]
    for one in loads:
        one.start()
    for one, then in zip(loads, stores):
        one.wait()
        then.start()
    for one in stores:
        one.wait()


def copied(arrays):
    count = len(arrays)
    return pl.pallas_call(
        functools.partial(copy_kernel, count),
        out_shape=tuple(jax.ShapeDtypeStruct(a.shape, a.dtype) for a in arrays),
        in_specs=[pl.BlockSpec(memory_space=pl.ANY)] * count,
        out_specs=(pl.BlockSpec(memory_space=pl.ANY),) * count,
        scratch_shapes=[pltpu.VMEM(a.shape, a.dtype) for a in arrays]
        + [pltpu.SemaphoreType.DMA((2, count))],
        compiler_params=pltpu.CompilerParams(vmem_limit_bytes=VMEM_LIMIT),
    )(*arrays)


def line_body(
    n_gr, n_fs, n_tp,
    prompt, train_gate, train_up, train_down, train_shared_gate, train_shared_up,
    train_shared_down, norm_gain, expert_ids, route_weight,
):
    experts, cols, hid = train_gate.shape
    rows, width = prompt.shape
    full, parts, sides = n_gr * n_fs, 2, n_tp // CORES
    sub, wide_hid = rows // parts, n_tp * hid
    bf16 = jnp.bfloat16
    f32 = jnp.float32
    hbm = pl.BlockSpec(memory_space=pl.ANY)
    dma = pltpu.SemaphoreType.DMA
    shape = jax.ShapeDtypeStruct
    outs = pl.pallas_call(
        functools.partial(line_kernel, n_gr, n_fs, n_tp, parts),
        out_shape=(
            shape((width, wide_hid), bf16),
            shape((width, wide_hid), bf16),
            shape((wide_hid, width), bf16),
            shape((hid, width), bf16),
            shape((hid, width), bf16),
            shape((hid, width), bf16),
            shape((parts, sub, width), bf16),
        ),
        in_specs=[hbm] * 10,
        out_specs=(hbm,) * 7,
        scratch_shapes=[
            pltpu.VMEM((rows, width), bf16),
            pltpu.VMEM((experts, hid, cols), f32),
            pltpu.VMEM((experts, hid, cols), f32),
            pltpu.VMEM((experts, hid, cols), f32),
            pltpu.VMEM((hid, cols), f32),
            pltpu.VMEM((hid, cols), f32),
            pltpu.VMEM((hid, cols), f32),
            pltpu.VMEM((1, cols), f32),
            pltpu.VMEM((expert_ids.shape[1], rows), jnp.int32),
            pltpu.VMEM((expert_ids.shape[1], rows), f32),
            pltpu.VMEM((n_fs, parts, sub, width), bf16),
            pltpu.VMEM((n_fs, experts, rows), f32),
            pltpu.VMEM((n_fs, CORES, sides, 3, hid, cols), bf16),
            pltpu.VMEM((full, CORES, sides, 3, wide_hid, cols), bf16),
            pltpu.VMEM((3, hid, cols), bf16),
            pltpu.VMEM((3, wide_hid, width), bf16),
            pltpu.VMEM((width, wide_hid), bf16),
            pltpu.VMEM((width, wide_hid), bf16),
            pltpu.VMEM((n_tp, n_fs * rows, 2 * wide_hid), f32),
            pltpu.VMEM((n_tp, rows, wide_hid), bf16),
            pltpu.VMEM((rows, width), f32),
            pltpu.VMEM((parts, sub, width), bf16),
            pltpu.VMEM((n_fs, parts, sub, width), bf16),
            pltpu.VMEM((n_fs, parts, sub, width), bf16),
            pltpu.VMEM((n_fs, parts, sub, width), bf16),
            dma((n_fs, parts)), dma((n_fs,)), dma((full * n_tp,)), dma((full * n_tp,)),
            dma((n_tp,)), dma((full,)), dma((n_fs, parts)), dma((n_fs, parts)),
            dma((2, n_fs, CORES)), dma((2 * n_fs, parts + 1)), dma((n_fs * CORES,)),
            dma((n_fs * CORES,)), dma((n_fs,)), dma((n_fs,)), dma((full,)),
            dma((2 * n_fs,)), dma((n_fs,)), dma((full,)), dma((2,)),
            dma((n_fs, parts)), dma((n_fs, parts)),
            dma((2 + parts,)), dma((4, full)), dma((10,)),
        ],
        compiler_params=pltpu.CompilerParams(
            collective_id=0, has_side_effects=True, vmem_limit_bytes=VMEM_LIMIT
        ),
    )(
        prompt, train_gate.transpose(0, 2, 1), train_up.transpose(0, 2, 1), train_down,
        train_shared_gate.T, train_shared_up.T, train_shared_down, norm_gain[None, :],
        expert_ids.T, route_weight.T,
    )
    serve_gate, serve_up, serve_down, s_gate, s_up, s_down, mixed_out = copied(outs)
    return (
        serve_gate[None], serve_up[None], serve_down[None],
        s_gate.T, s_up.T, s_down, mixed_out.reshape(rows, width),
    )


def regroup(stacked, lowered):
    stacked = lax.all_to_all(
        lax.all_to_all(stacked, "fs", split_axis=0, concat_axis=2, tiled=True),
        "tp",
        split_axis=0,
        concat_axis=3,
        tiled=True,
    )
    lowered = lax.all_to_all(
        lax.all_to_all(lowered, "fs", split_axis=0, concat_axis=2, tiled=True),
        "tp",
        split_axis=0,
        concat_axis=1,
        tiled=True,
    )
    return (stacked, lowered)


def body(
    prompt,
    train_gate,
    train_up,
    train_down,
    train_shared_gate,
    train_shared_up,
    train_shared_down,
    norm_gain,
    expert_ids,
    route_weight,
):
    gain_col = norm_gain[:, None]
    stacked = jnp.stack((train_gate * gain_col[None], train_up * gain_col[None]), axis=1).astype(
        jnp.bfloat16
    )
    lowered = train_down.astype(jnp.bfloat16)
    stacked, lowered = regroup(stacked, lowered)
    stacked, lowered = (
        lax.all_gather(stacked, "gr", axis=2, tiled=True),
        lax.all_gather(lowered, "gr", axis=2, tiled=True),
    )
    serve_gate = stacked[:, 0]
    serve_up = stacked[:, 1]
    serve_shared_gate, serve_shared_up, serve_shared_down = (
        lax.all_gather(
            (train_shared_gate * gain_col).astype(jnp.bfloat16), ("gr", "fs"), axis=0, tiled=True
        ),
        lax.all_gather(
            (train_shared_up * gain_col).astype(jnp.bfloat16), ("gr", "fs"), axis=0, tiled=True
        ),
        lax.all_gather(train_shared_down.astype(jnp.bfloat16), ("gr", "fs"), axis=1, tiled=True),
    )
    widened = prompt.astype(jnp.float32)
    normed = (
        widened * lax.rsqrt(jnp.mean(widened * widened, axis=-1, keepdims=True) + eps_norm)
    ).astype(jnp.bfloat16)
    block_rows = lax.all_gather(normed, "tp", axis=0, tiled=True)
    gate_val = jnp.dot(block_rows, serve_shared_gate, preferred_element_type=jnp.float32)
    up_val = jnp.dot(block_rows, serve_shared_up, preferred_element_type=jnp.float32)
    shared_act = (jax.nn.silu(gate_val) * up_val).astype(jnp.bfloat16)
    shared_sum = lax.psum_scatter(
        jnp.dot(shared_act, serve_shared_down, preferred_element_type=jnp.float32).astype(
            jnp.bfloat16
        ),
        "tp",
        scatter_dimension=0,
        tiled=True,
    ).astype(jnp.float32)
    row_count = prompt.shape[0]
    top_count = expert_ids.shape[1]
    model_width = prompt.shape[1]
    expert_count = lax.axis_size("fs") * lax.axis_size("tp")
    capacity = row_count * top_count // expert_count + 1
    flat_ids = expert_ids.reshape(-1)
    onehot = (flat_ids[:, None] == jnp.arange(expert_count, dtype=jnp.int32)[None, :]).astype(
        jnp.int32
    )
    earlier = jnp.cumsum(onehot, axis=0) - onehot
    places = jnp.sum(earlier * onehot, axis=1)
    slot_ids = (flat_ids * capacity + places).reshape(row_count, top_count)
    slot_range = jnp.arange(expert_count * capacity, dtype=jnp.int32)
    dispatch = jnp.any(slot_range[:, None, None] == slot_ids[None, :, :], axis=-1).astype(
        jnp.bfloat16
    )
    outgoing = jnp.dot(dispatch, normed, preferred_element_type=jnp.float32).astype(jnp.bfloat16)
    outgoing = outgoing.reshape(expert_count, capacity, model_width)
    arrived = lax.all_to_all(outgoing, ("fs", "tp"), split_axis=0, concat_axis=0, tiled=True)
    source_count, slot_count, width_here = arrived.shape
    arrived_rows = arrived.reshape(source_count * slot_count, width_here)
    gate_val = jnp.dot(arrived_rows, serve_gate[0], preferred_element_type=jnp.float32)
    up_val = jnp.dot(arrived_rows, serve_up[0], preferred_element_type=jnp.float32)
    hidden = (jax.nn.silu(gate_val) * up_val).astype(jnp.bfloat16)
    result = jnp.dot(hidden, lowered[0], preferred_element_type=jnp.float32).astype(jnp.bfloat16)
    result = result.reshape(source_count, slot_count, width_here)
    returned = lax.all_to_all(result, ("fs", "tp"), split_axis=0, concat_axis=0, tiled=True)
    picked = returned.reshape(expert_count * capacity, model_width)[slot_ids]
    routed = jnp.sum(route_weight[:, :, None] * picked.astype(jnp.float32), axis=1)
    mixed_out = (routed + shared_sum).astype(jnp.bfloat16)
    return (
        serve_gate,
        serve_up,
        lowered,
        serve_shared_gate,
        serve_shared_up,
        serve_shared_down,
        mixed_out,
    )


def solution(mesh):
    placed = (
        P(("gr", "fs", "tp"), None),
        P(None, ("gr", "fs"), "tp"),
        P(None, ("gr", "fs"), "tp"),
        P(None, "tp", ("gr", "fs")),
        P(("gr", "fs"), "tp"),
        P(("gr", "fs"), "tp"),
        P("tp", ("gr", "fs")),
        P(("gr", "fs")),
        P(("gr", "fs", "tp"), None),
        P(("gr", "fs", "tp"), None),
    )
    n_gr, n_fs, n_tp = (mesh.shape[name] for name in ("gr", "fs", "tp"))

    def chosen(prompt, train_gate, *rest):
        rows, width = prompt.shape
        experts, cols, hid = train_gate.shape
        held = n_fs * n_tp * n_gr * CORES * 3 * hid * cols * 4 + 4 * n_fs * prompt.size * 2
        fits = n_gr == 2 and n_tp == 2 * CORES and n_fs % 2 == 0 and held < VMEM_PLAN
        even = experts == n_fs * n_tp and cols * n_gr * n_fs == width and rows == 128
        if fits and even and hid % (16 * n_fs) == 0 and cols % 128 == 0:
            return line_body(n_gr, n_fs, n_tp, prompt, train_gate, *rest)
        return body(prompt, train_gate, *rest)

    return jax.shard_map(
        chosen,
        mesh=mesh,
        in_specs=placed,
        out_specs=(
            P(("fs", "tp"), None, None),
            P(("fs", "tp"), None, None),
            P(("fs", "tp"), None, None),
            P(None, "tp"),
            P(None, "tp"),
            P("tp", None),
            P(("gr", "fs", "tp"), None),
        ),
        check_vma=False,
    )
```

time: 141 us -> 118 us (0.84)
  Pallas kernels: 140 us -> 116 us
    pallas_call x1, Pallas kernels: 136 us -> 113 us  [line_body(): pl.pallas_call(functools.partial(line_kernel, n_gr, n_fs, n_tp, parts), o...]
where the time goes in v2:
time: 118 us; the launch traced here: 117 us
  Pallas kernels  116 us (98%)
    pallas_call x1, Pallas kernels, line_body(): pl.pallas_call(functools.partial(line_kernel, n_gr, n_fs, n_tp, parts), o...  113 us
    pallas_call x1, Pallas kernels, copied(): pl.pallas_call(functools.partial(copy_kernel, count), out_shape=tuple((ja...  3.44 us

profile of v2, /device:TPU:0, one launch (start us, length us, event | category | flops | bytes accessed | tf_op | source)
XLA Modules:
  0.0 117.0 jit_solution(15998824445213633162)
XLA Ops:
  0.6 112.9 %shard_map.153 = (bf16[2048,256]{1,0:T(8,128)(2,1)}, bf16[2048,256]{1,0:T(8,128)(2,1)}, bf16[256,2048]{1,0:T(8,128)(2,1)}, bf16[64,2048]{1,0:T(8,128)(2,1)}, bf1...) custom-call(bf16[128,2048]{1,0:T(8,128)(2,1)} %p_hbm.1, f32[16,64,256]{2,1,0:T(8,128)} %bitcast.13, ...), custom_call_target="tpu_custom_call" | custom-call | tf_op jit(solution)/shard_map/pallas_call | solution.py:558
  113.6 3.4 %shard_map.154 = (bf16[2048,256]{1,0:T(8,128)(2,1)}, bf16[2048,256]{1,0:T(8,128)(2,1)}, bf16[256,2048]{1,0:T(8,128)(2,1)}, bf16[64,2048]{1,0:T(8,128)(2,1)}, bf1...) custom-call(bf16[2048,256]{1,0:T(8,128)(2,1)} %get-tuple-element.21.refs_0_, ...), custom_call_target="tpu_custom_call" | custom-call | tf_op jit(solution)/shard_map/pallas_call | solution.py:533

commit v3 on v2

--- a/solution.py
+++ b/solution.py
@@ -10,6 +10,7 @@
 eps_norm = 1e-06
 MESH = pl.DeviceIdType.MESH
 CORES = 2
+PARTS = 4
 VMEM_PLAN = 40 * 2**20
 VMEM_LIMIT = 60 * 2**20
 
@@ -59,15 +60,23 @@
         fall = jnp.where(f > at, n_fs - f, n_fs - 1 - f)
         return jnp.where(f == at, 0, jnp.where(at < n_fs // 2, rise, fall))
 
-    ins = [
-        pltpu.make_async_copy(src, dst, in_sem.at[i])
+    first = pltpu.make_async_copy(gain_hbm, gain_ref, in_sem.at[0])
+    first.start()
+    heavy = []
+    for p in range(n_fs):
+        at = pl.ds(order[p] * n_tp, n_tp)
+        heavy.append([
+            pltpu.make_async_copy(src.at[at], dst.at[at], in_sem.at[1 + 3 * p + i])
+            for i, (src, dst) in enumerate(((gt_hbm, gt_ref), (ut_hbm, ut_ref), (dn_hbm, dn_ref)))
+        ])
+    light = [
+        pltpu.make_async_copy(src, dst, in_sem.at[1 + 3 * n_fs + i])
         for i, (src, dst) in enumerate((
-            (gain_hbm, gain_ref), (gt_hbm, gt_ref), (ut_hbm, ut_ref), (dn_hbm, dn_ref),
             (tsg_hbm, sg_ref), (tsu_hbm, su_ref), (tsd_hbm, sd_ref), (p_hbm, p_ref),
             (ids_hbm, ids_ref), (rw_hbm, rw_ref),
         ))
     ]
-    for one in ins:
+    for one in sum(heavy, []) + light:
         one.start()
 
     barrier = pltpu.get_barrier_semaphore()
@@ -82,18 +91,20 @@
     greet(to_x)
     greet(to_y)
 
-    for one in ins[:4]:
-        one.wait()
+    first.wait()
     gain = gain_ref[...]
 
-    def cast(i, carry):
-        f, t = i // n_tp, i % n_tp
-        e_in[f, t % CORES, t // CORES, 0] = (gt_ref[i] * gain).astype(jnp.bfloat16)
-        e_in[f, t % CORES, t // CORES, 1] = (ut_ref[i] * gain).astype(jnp.bfloat16)
-        e_in[f, t % CORES, t // CORES, 2] = dn_ref[i].astype(jnp.bfloat16)
-        return carry
-
-    lax.fori_loop(0, n_fs * n_tp, cast, 0)
+    def cast(p):
+        for one in heavy[p]:
+            one.wait()
+        f = order[p]
+        for t in range(n_tp):
+            i = f * n_tp + t
+            e_in[f, t % CORES, t // CORES, 0] = (gt_ref[i] * gain).astype(jnp.bfloat16)
+            e_in[f, t % CORES, t // CORES, 1] = (ut_ref[i] * gain).astype(jnp.bfloat16)
+            e_in[f, t % CORES, t // CORES, 2] = dn_ref[i].astype(jnp.bfloat16)
+
+    cast(0)
     pl.semaphore_wait(barrier, n_fs * CORES + 1)
 
     def remote(src, dst, send, recv, where):
@@ -110,8 +121,9 @@
         else:
             pl.when(cond)(f)
 
-    def go(cond, copies):
-        pending.append((cond, copies))
+    def go(cond, copies, drain=True):
+        if drain:
+            pending.append((cond, copies))
 
         def start():
             for one in copies:
@@ -119,6 +131,9 @@
 
         when(cond, start)
 
+    def drain(cond, ref, sem):
+        pending.append((cond, [remote(ref, ref, sem, sc.at[0], to_c)]))
+
     def slab(g, f, t, core):
         at = pl.ds(pl.multiple_of(t * hid, hid), hid)
         return w_all.at[g * n_fs + f, core, :, :, at, :]
@@ -126,31 +141,33 @@
     def got(g, f, t):
         return er.at[(g * n_fs + f) * n_tp + t]
 
-    def send_expert(d, i):
+    def send_expert(p, i):
+        f = order[p]
         core = c if i == 0 else c_other
-        for way in (0, 1):
-            f = z + d if way == 0 else z - d
-            there = f < n_fs if way == 0 else f >= 0
-            go(there, [remote(
-                e_in.at[f, core], slab(gr, z, tp, core), zs.at[way, d, i],
-                got(gr, z, tp), dev(gr, f, y * CORES + core),
-            )])
+        go(None, [remote(
+            e_in.at[f, core], slab(gr, z, tp, core), zs.at[1 if p == 1 else 2],
+            got(gr, z, tp), dev(gr, f, y * CORES + core),
+        )], False)
 
     def wait_slab(g, f, t):
-        remote(e_in.at[0, 0], slab(g, f, t, c), zs.at[0, 0, 0], got(g, f, t), to_x).wait_recv()
+        remote(e_in.at[0, 0], slab(g, f, t, c), zs.at[0], got(g, f, t), to_x).wait_recv()
 
     def pass_slab(g, f, t, sem, where, src=None):
         place = slab(g, f, t, c)
         return remote(place if src is None else src, place, sem, got(g, f, t), where)
 
-    def row_copies(f, h, sem, way):
+    def send_rows(cond, f, h, slot, way):
         to = z + 1 if way == 0 else z - 1
         here, there = place(f, z), place(f, to)
         where = dev(gr, to, tp)
-        copies = [remote(x_all.at[here, h], x_all.at[there, h], sem.at[h], xr.at[f, h], where)]
+        sem = zd.at[slot, 0]
+        go(cond, [remote(x_all.at[here, h], x_all.at[there, h], sem, xr.at[f, h], where)], False)
         if h == 0:
-            copies.append(remote(t_all.at[f], t_all.at[f], sem.at[parts], tr.at[f], where))
-        return copies
+            drain(cond, x_all.at[0], sem)
+            go(cond, [remote(t_all.at[f], t_all.at[f], zd.at[slot, 1], tr.at[f], where)])
+
+    def s_slice(t):
+        return s_all.at[:, pl.ds(pl.multiple_of(t * hid, hid), hid), :]
 
     def s_slab(g, f, t):
         lanes = pl.ds(pl.multiple_of((g * n_fs + f) * cols, 128), cols)
@@ -158,21 +175,36 @@
 
     def s_copy(src, g, f, sem, where, t=tp):
         src = s_slab(g, f, t) if src is None else src
-        return remote(src, s_slab(g, f, t), sem, sr.at[(g * n_fs + f) * n_tp + t], where)
+        recv = sr.at[full] if where is to_y else sr.at[g * n_fs + f]
+        return remote(src, s_slab(g, f, t), sem, recv, where)
 
     mine = e_in.at[z, c]
     go(None, [remote(
-        e_in.at[z, c_other], slab(gr, z, tp, c_other), zs.at[0, 0, 1], got(gr, z, tp), to_c
+        e_in.at[z, c_other], slab(gr, z, tp, c_other), zs.at[0], got(gr, z, tp), to_c
     )])
-    go(None, [pass_slab(gr, z, tp, xs.at[z * CORES + c], to_x, mine)])
-    go(None, [pass_slab(gr, z, tp, ys.at[z * CORES + c], to_y, mine)])
+    go(None, [pass_slab(gr, z, tp, xs.at[0], to_x, mine)], False)
+    go(None, [pass_slab(gr, z, tp, ys.at[0], to_y, mine)], False)
+    cast(1)
     for i in range(CORES):
-        for d in range(1, n_fs):
-            send_expert(d, i)
+        send_expert(1, i)
+    for p in range(2, n_fs):
+        cast(p)
+    for i in range(CORES):
+        for p in range(2, n_fs):
+            send_expert(p, i)
+    drain(None, w_all.at[0, 0, 0], zs.at[1])
+    drain(None, w_all.at[0, 0], zs.at[2])
+    drain(None, w_all.at[0], xs.at[0])
+    drain(None, w_all.at[0], ys.at[0])
+    drain(None, w_all.at[0, 0], xd.at[0])
+    drain(None, w_all.at[0, 0], yd.at[0])
+    drain(None, w_all.at[0 : full // 2], fs_.at[0])
+    drain(None, w_all.at[0, 0, 0], sx.at[0])
+    drain(None, s_slice(tp), sy.at[0])
     near_slab = pltpu.make_async_copy(mine, slab(gr, z, tp, c), loc.at[0])
     near_slab.start()
 
-    for one in ins[4:]:
+    for one in light:
         one.wait()
     s_in[0] = (sg_ref[...] * gain).astype(jnp.bfloat16)
     s_in[1] = (su_ref[...] * gain).astype(jnp.bfloat16)
@@ -195,7 +227,7 @@
         for h in range(parts):
             for way in (0, 1):
                 there = has_up if way == 0 else has_down
-                go(there & cond, row_copies(z, h, zd.at[way], way))
+                send_rows(there & cond, z, h, way, way)
         go(has_up & cond, [s_copy(s_in, gr, z, ss.at[0], up)])
         go(has_down & cond, [s_copy(s_in, gr, z, ss.at[1], down)])
 
@@ -206,45 +238,62 @@
         core = c if i == 0 else c_other
         t = y * CORES + core
         wait_slab(gr, f, t)
-        go(None, [pass_slab(gr, f, t, xs.at[f * CORES + core], to_x)])
-        go(None, [pass_slab(gr, f, t, ys.at[f * CORES + core], to_y)])
+        go(None, [pass_slab(gr, f, t, xs.at[0], to_x)], False)
+        go(None, [pass_slab(gr, f, t, ys.at[0], to_y)], False)
 
     def result_copies(k):
         at = pl.ds(pl.multiple_of(k * cols, 128), cols)
         return [
-            pltpu.make_async_copy(gate_out.at[at, :], gate_hbm.at[at, :], res_sem.at[0, k]),
-            pltpu.make_async_copy(up_out.at[at, :], up_hbm.at[at, :], res_sem.at[1, k]),
-            pltpu.make_async_copy(w_all.at[k, c, y, 2], down_hbm.at[:, at], res_sem.at[2, k]),
+            pltpu.make_async_copy(gate_out.at[at, :], gate_hbm.at[at, :], res_sem.at[0]),
+            pltpu.make_async_copy(up_out.at[at, :], up_hbm.at[at, :], res_sem.at[1]),
+            pltpu.make_async_copy(w_all.at[k, c, y, 2], down_hbm.at[:, at], res_sem.at[2]),
         ]
 
-    def give(g, f):
+    half = wide_hid // sides
+
+    def half_copy(k, core, part_of):
+        at = pl.ds(pl.multiple_of(part_of * half, half), half)
+        place_of = w_all.at[k, core, :, :, at, :]
+        return remote(place_of, place_of, fs_.at[0], fr.at[k, part_of], to_c)
+
+    def give(g, f, part_of):
+        go(None, [half_copy(g * n_fs + f, c, part_of)], False)
+
+    def turn(g, f):
         k = g * n_fs + f
-        go(None, [remote(w_all.at[k, c], w_all.at[k, c], fs_.at[k], fr.at[k], to_c)])
         at = pl.ds(pl.multiple_of(k * cols, 128), cols)
         gate_out[at, :] = w_all[k, c, y, 0].T
         up_out[at, :] = w_all[k, c, y, 1].T
         for one in result_copies(k):
             one.start()
 
-    def side(p, core):
+    def side(p, i):
         f = order[p]
+        core = c if i == 0 else c_other
         wait_slab(x_peer, f, y * CORES + core)
-        if core == 0:
-            go(None, [pass_slab(x_peer, f, y * CORES, yd.at[f], to_y)])
+        if (p + i) % 2 == 0:
+            go(None, [pass_slab(x_peer, f, y * CORES + core, yd.at[0], to_y)], False)
         wait_slab(gr, f, y_other * CORES + core)
-        if core == 1:
-            go(None, [pass_slab(gr, f, y_other * CORES + 1, xd.at[f], to_x)])
+        if (p + i) % 2 == 1:
+            go(None, [pass_slab(gr, f, y_other * CORES + core, xd.at[0], to_x)], False)
+        if i == CORES - 1:
+            give(x_peer, f, y)
 
     def column(p):
         if p == 0:
             near_slab.wait()
-        give(gr, order[p])
+        give(gr, order[p], y)
+        give(gr, order[p], y_other)
+        turn(gr, order[p])
 
     def corner(p):
         f = order[p]
         for core in range(CORES):
             wait_slab(x_peer, f, y_other * CORES + core)
-        give(x_peer, f)
+        give(x_peer, f, y_other)
+
+    def corner_turn(p):
+        turn(x_peer, order[p])
 
     def row_part(p, h, most=None):
         f = order[p]
@@ -256,8 +305,8 @@
 
         when(most, arrive)
         if most is inner:
-            go((f < z) & inner, row_copies(f, h, zd.at[1 + p], 0))
-            go((f > z) & inner, row_copies(f, h, zd.at[n_fs + p], 1))
+            send_rows((f < z) & inner, f, h, 1 + p, 0)
+            send_rows((f > z) & inner, f, h, n_fs + p, 1)
 
     def wait_shared(g, f, t):
         s_copy(None, g, f, sx.at[0], to_x, t).wait_recv()
@@ -270,30 +319,37 @@
             go((f < z) & has_up & most, [s_copy(src, gr, f, ss.at[1 + p], up)])
             go((f > z) & has_down & most, [s_copy(src, gr, f, ss.at[n_fs + p], down)])
         most = None if most is True else most
-        go(most, [s_copy(src, gr, f, sx.at[f], to_x)])
-        go(most, [s_copy(src, gr, f, sy.at[gr * n_fs + f], to_y)])
+        go(most, [s_copy(src, gr, f, sx.at[0], to_x)], False)
+        go(most, [s_copy(src, gr, f, sy.at[0], to_y)], False)
 
     def shared_x(p):
         f = order[p]
         wait_shared(x_peer, f, tp)
-        go(None, [s_copy(None, x_peer, f, sy.at[x_peer * n_fs + f], to_y)])
+        go(None, [s_copy(None, x_peer, f, sy.at[0], to_y)], False)
 
     def nt(a, b):
         return lax.dot_general(a, b, (((1,), (1,)), ((), ())), preferred_element_type=jnp.float32)
 
-    def step(g, f, first=False):
-        k = g * n_fs + f
-        remote(w_all.at[k, c], w_all.at[k, c_other], fs_.at[k], fr.at[k], to_c).wait_recv()
+    def arrived(g, f):
+        for side_of in range(sides):
+            half_copy(g * n_fs + f, c_other, side_of).wait_recv()
+
+    def add(k, lo, hi, first):
         at = pl.ds(pl.multiple_of(k * cols, 128), cols)
-        some = (n_fs - 1) * rows
-        lhs = x_all[0 : n_fs - 1, :, :, at].reshape(some, cols)
+        lhs = x_all[lo:hi, :, :, at].reshape((hi - lo) * rows, cols)
+        here = slice(lo * rows, hi * rows)
         for s in range(n_tp):
             w = w_all[k, s // sides, s % sides, 0:2].reshape(2 * wide_hid, cols)
             val = nt(lhs, w)
-            acc[s, 0:some] = val if first else acc[s, 0:some] + val
-
-    def late():
-        lhs = x_all[n_fs - 1].reshape(rows, width)
+            acc[s, here] = val if first else acc[s, here] + val
+
+    def step(g, f, lo, hi, first=False):
+        add(g * n_fs + f, lo, hi, first)
+
+    def late(lo, hi):
+        some = (hi - lo) * sub
+        lhs = x_all[n_fs - 1, lo:hi].reshape(some, width)
+        here = (n_fs - 1) * rows + lo * sub
 
         def one(s, carry):
             total = None
@@ -301,19 +357,16 @@
                 w = w_all[k, s // sides, s % sides, 0:2].reshape(2 * wide_hid, cols)
                 val = nt(lhs[:, k * cols : (k + 1) * cols], w)
                 total = val if total is None else total + val
-            acc[s, (n_fs - 1) * rows :] = total
+            acc[s, here : here + some] = total
             return carry
 
         lax.fori_loop(0, n_tp, one, 0)
-
-    def s_slice(t):
-        return s_all.at[:, pl.ds(pl.multiple_of(t * hid, hid), hid), :]
 
     def s_whole(t, i):
         return remote(s_slice(t), s_slice(t), sd.at[i], sc.at[t], to_c)
 
     s_results = [
-        pltpu.make_async_copy(s_slice(tp).at[i], dst, res_sem.at[3, i])
+        pltpu.make_async_copy(s_slice(tp).at[i], dst, res_sem.at[3 + i])
         for i, dst in enumerate((sg_hbm, su_hbm, sd_hbm))
     ]
     t_y = y_other * CORES + c
@@ -323,9 +376,7 @@
         go(None, [s_whole(tp, 0)])
         for one in s_results:
             one.start()
-        for g in range(n_gr):
-            for f in range(n_fs):
-                wait_shared(g, f, t_y)
+        remote(s_slice(t_y), s_slice(t_y), sy.at[0], sr.at[full], to_y).wait_recv()
         go(None, [s_whole(t_y, 1)])
 
     def shared_act():
@@ -348,29 +399,38 @@
     def then(f, *args):
         stages.append((f, args))
 
+    def only(cond, f, *args):
+        @functools.wraps(f)
+        def run(*given):
+            pl.when(cond)(lambda: f(*given))
+
+        stages.append((run, args))
+
     def wide(v):
         return v.astype(jnp.float32)
 
     def u_copy(t, h):
-        return remote(part.at[t, h], ru.at[t, h], us.at[t, h], ur.at[t, h], up)
+        return remote(part.at[t, h], ru.at[t, h], us.at[t], ur.at[t, h], up)
 
     def d_copy(t, h):
-        return remote(part.at[t, h], rd.at[t, h], ds_.at[t, h], dr.at[t, h], down)
+        return remote(part.at[t, h], rd.at[t, h], ds_.at[t], dr.at[t, h], down)
 
     def when_way(t, ahead, behind):
         pl.when(t > z)(ahead)
         pl.when(t < z)(behind)
 
-    def block(p):
+    def block(p, lo=0, hi=parts):
         t = order[p]
-        here = slice(p * rows, (p + 1) * rows)
+        some, skip = (hi - lo) * sub, lo * sub
+        here = slice(p * rows + skip, p * rows + skip + some)
 
         for s in range(n_tp):
             e = z * n_tp + (s % sides) * CORES + s // sides
-            scale = jnp.broadcast_to(t_all[t, pl.ds(e, 1), :], (rows, rows)).T[:, :1]
+            scale = jnp.broadcast_to(t_all[t, pl.ds(e, 1), :], (rows, rows)).T
+            scale = scale[skip : skip + some, :1]
             val = acc[s, here, :]
             val = jax.nn.silu(val[:, :wide_hid]) * val[:, wide_hid:] * scale
-            act[s] = val.astype(jnp.bfloat16)
+            act[s, 0:some] = val.astype(jnp.bfloat16)
 
         group = 4
 
@@ -381,22 +441,23 @@
                 total = None
                 for s in range(n_tp):
                     val = jnp.dot(
-                        act[s], w_all[k, s // sides, s % sides, 2],
+                        act[s, 0:some], w_all[k, s // sides, s % sides, 2],
                         preferred_element_type=jnp.float32,
                     )
                     total = val if total is None else total + val
-                part[t, :, :, at] = total.astype(jnp.bfloat16).reshape(parts, sub, cols)
+                total = total.astype(jnp.bfloat16)
+                part[t, lo:hi, :, at] = total.reshape(hi - lo, sub, cols)
             return carry
 
         lax.fori_loop(0, full // group, columns, 0)
         if p:
-            for h in range(parts):
-                pl.when((t > z) & jnp.logical_not(has_down))(lambda: u_copy(t, h).start())
-                pl.when((t < z) & jnp.logical_not(has_up))(lambda: d_copy(t, h).start())
-
-    def chain(p):
+            for g in range(lo, hi):
+                pl.when((t > z) & jnp.logical_not(has_down))(lambda g=g: u_copy(t, g).start())
+                pl.when((t < z) & jnp.logical_not(has_up))(lambda g=g: d_copy(t, g).start())
+
+    def chain(p, lo=0, hi=parts):
         t = order[p]
-        for h in range(parts):
+        for h in range(lo, hi):
             for copy, arrived, cond in (
                 (u_copy, ru, (t > z) & has_down), (d_copy, rd, (t < z) & has_up)
             ):
@@ -438,60 +499,97 @@
 
         mixed_copy(h).start()
 
-    last = n_fs - 1
+    last, half_way = n_fs - 1, parts // 2
     then(own, 0, 1)
-    for i in range(CORES):
-        for p in range(1, n_fs):
-            then(own, p, i)
-            if i == 0 and p == last:
-                then(side, 0, 0)
-                then(side, 0, 1)
-                then(column, 0)
-    for p in range(1, last):
+    then(own, 1, 0)
+    then(own, 1, 1)
+    then(side, 0, 0)
+    then(side, 0, 1)
+    then(column, 0)
+    for p in range(2, n_fs):
+        then(own, p, 0)
+    then(side, 1, 0)
+    then(side, 1, 1)
+    then(column, 1)
+    for p in range(2, n_fs):
+        then(own, p, 1)
+    for p in range(2, n_fs):
         then(side, p, 0)
-        then(side, p, 1)
-        then(column, p)
+    for h in range(half_way):
+        then(row_part, 1, h, inner)
+    then(row_part, 2, 0, inner)
+    for h in range(half_way, parts):
+        then(row_part, 1, h, inner)
+    then(side, 2, 1)
+    for h in range(1, parts - 1):
+        then(row_part, 2, h, inner)
+    then(side, last, 1)
+    then(row_part, 2, parts - 1, inner)
+    then(column, 2)
+    then(column, last)
+    then(corner, 0)
+    then(corner, 1)
     for h in range(parts):
-        for p in range(1, last):
-            then(row_part, p, h, inner)
-    then(corner, 0)
-    then(side, last, 0)
-    then(side, last, 1)
-    then(column, last)
+        then(row_part, 1, h, outer)
     then(shared, 0)
-    for p in range(1, last):
-        for h in range(parts):
-            then(row_part, p, h, outer)
-        then(shared, p, inner)
-    then(corner, 1)
+    then(shared, 1, outer)
+    then(corner_turn, 0)
+    then(corner_turn, 1)
     for p in range(n_fs):
-        then(step, gr, order[p], p == 0)
+        then(arrived, gr, order[p])
+        then(step, gr, order[p], 0, 2, p == 0)
     for p in range(2):
-        then(step, x_peer, order[p])
-    then(shared, 1, outer)
+        then(arrived, x_peer, order[p])
+        then(step, x_peer, order[p], 0, 2)
+    for h in range(half_way):
+        then(row_part, last, h, inner)
+    for h in range(parts):
+        then(row_part, 2, h, outer)
+    then(step, gr, order[0], 2, 3, True)
+    then(step, gr, order[1], 2, 3)
+    then(corner, 2)
+    for h in range(half_way, parts - 1):
+        then(row_part, last, h, inner)
     for p in range(2, n_fs):
-        then(row_part, last, p - 2, inner)
-        then(corner, p)
-        then(step, x_peer, order[p])
+        then(step, gr, order[p], 2, 3)
+    then(row_part, last, parts - 1, inner)
+    then(shared, 1, inner)
+    then(shared, 2, inner)
+    then(corner, last)
+    for p in range(2):
+        then(step, x_peer, order[p], 2, 3)
+    for p in range(2, n_fs):
+        then(arrived, x_peer, order[p])
+        then(step, x_peer, order[p], 0, 3)
     then(block, last - 1)
+    only(inner, late, 0, parts)
+    only(inner, block, last, 0, parts)
+    for lo, hi in ((0, half_way), (half_way, parts)):
+        for h in range(lo, hi):
+            then(row_part, last, h, outer)
+        only(outer, late, lo, hi)
+        only(outer, block, last, lo, hi)
     then(shared, last, inner)
-    for h in range(parts):
-        then(row_part, last, h, outer)
-    then(late)
-    then(block, last)
+    then(chain, last - 1, 0, half_way)
+    then(block, 1)
+    then(shared, 2, outer)
+    then(block, 0)
+    then(chain, last - 1, half_way, parts)
+    then(corner_turn, 2)
+    then(corner_turn, last)
+    then(shared, last, outer)
+    then(shared_x, 0)
+    then(shared_x, 1)
+    then(chain, last, 0, half_way)
+    then(shared_x, 2)
+    then(shared_x, last)
+    then(chain, last, half_way, parts)
     for p in range(1, last - 1):
-        then(block, p)
-    for p in range(2, n_fs):
-        then(shared, p, outer)
-    then(block, 0)
-    then(chain, last - 1)
-    for p in range(n_fs):
-        then(shared_x, p)
-    then(chain, last)
+        then(chain, p, 0, half_way)
     then(shared_give)
+    for p in range(1, last - 1):
+        then(chain, p, half_way, parts)
     then(shared_act)
-    for p in range(1, last - 1):
-        then(chain, p)
     for h in range(parts):
         then(finish, h)
 
@@ -504,15 +602,16 @@
             mixed_copy(h).wait()
         for one in s_results:
             one.wait()
-        for k in range(full):
-            for one in result_copies(k):
-                one.wait()
+        for i, (src, dst) in enumerate((
+            (gate_out, gate_hbm), (up_out, up_hbm), (gate_out, gate_hbm),
+        )):
+            pltpu.make_async_copy(src, dst, res_sem.at[i]).wait()
         for cond, copies in pending:
             when(cond, lambda copies=copies: [one.wait_send() for one in copies] and None)
-        for d in range(1, n_fs):
-            for h in range(parts):
-                pl.when(z + d < n_fs)(lambda d=d, h=h: u_copy(z + d, h).wait_send())
-                pl.when(z - d >= 0)(lambda d=d, h=h: d_copy(z - d, h).wait_send())
+        for t in range(n_fs):
+            whole = part.at[t]
+            pl.when(t > z)(lambda: remote(whole, whole, us.at[t], ur.at[t, 0], up).wait_send())
+            pl.when(t < z)(lambda: remote(whole, whole, ds_.at[t], dr.at[t, 0], down).wait_send())
 
 
 def copy_kernel(count, *refs):
@@ -548,7 +647,7 @@
 ):
     experts, cols, hid = train_gate.shape
     rows, width = prompt.shape
-    full, parts, sides = n_gr * n_fs, 2, n_tp // CORES
+    full, parts, sides = n_gr * n_fs, PARTS, n_tp // CORES
     sub, wide_hid = rows // parts, n_tp * hid
     bf16 = jnp.bfloat16
     f32 = jnp.float32
@@ -594,13 +693,12 @@
             pltpu.VMEM((n_fs, parts, sub, width), bf16),
             pltpu.VMEM((n_fs, parts, sub, width), bf16),
             pltpu.VMEM((n_fs, parts, sub, width), bf16),
-            dma((n_fs, parts)), dma((n_fs,)), dma((full * n_tp,)), dma((full * n_tp,)),
-            dma((n_tp,)), dma((full,)), dma((n_fs, parts)), dma((n_fs, parts)),
-            dma((2, n_fs, CORES)), dma((2 * n_fs, parts + 1)), dma((n_fs * CORES,)),
-            dma((n_fs * CORES,)), dma((n_fs,)), dma((n_fs,)), dma((full,)),
-            dma((2 * n_fs,)), dma((n_fs,)), dma((full,)), dma((2,)),
-            dma((n_fs, parts)), dma((n_fs, parts)),
-            dma((2 + parts,)), dma((4, full)), dma((10,)),
+            dma((n_fs, parts)), dma((n_fs,)), dma((full * n_tp,)), dma((full + 1,)),
+            dma((n_tp,)), dma((full, sides)), dma((n_fs, parts)), dma((n_fs, parts)),
+            dma((3,)), dma((2 * n_fs, 2)), dma((1,)), dma((1,)), dma((1,)), dma((1,)),
+            dma((1,)), dma((2 * n_fs,)), dma((1,)), dma((1,)), dma((2,)),
+            dma((n_fs,)), dma((n_fs,)),
+            dma((2 + parts,)), dma((6,)), dma((7 + 3 * n_fs,)),
         ],
         compiler_params=pltpu.CompilerParams(
             collective_id=0, has_side_effects=True, vmem_limit_bytes=VMEM_LIMIT

time: 118 us -> 109 us (0.924)
  Pallas kernels: 116 us -> 108 us
    pallas_call x1, Pallas kernels: 113 us -> 105 us  [line_body(): pl.pallas_call(functools.partial(line_kernel, n_gr, n_fs, n_tp, parts), o...]
where the time goes in v3:
time: 109 us
  Pallas kernels  108 us (99%)
    pallas_call x1, Pallas kernels, line_body(): pl.pallas_call(functools.partial(line_kernel, n_gr, n_fs, n_tp, parts), o...  105 us
    pallas_call x1, Pallas kernels, copied(): pl.pallas_call(functools.partial(copy_kernel, count), out_shape=tuple((ja...  3.44 us

profile of v3, /device:TPU:0, one launch (start us, length us, event | category | flops | bytes accessed | tf_op | source)
XLA Modules:
  0.0 109.0 jit_solution(6911352902606160897)
XLA Ops:
  0.6 104.9 %shard_map.153 = (bf16[2048,256]{1,0:T(8,128)(2,1)}, bf16[2048,256]{1,0:T(8,128)(2,1)}, bf16[256,2048]{1,0:T(8,128)(2,1)}, bf16[64,2048]{1,0:T(8,128)(2,1)}, bf1...) custom-call(bf16[128,2048]{1,0:T(8,128)(2,1)} %p_hbm.1, f32[16,64,256]{2,1,0:T(8,128)} %bitcast.13, ...), custom_call_target="tpu_custom_call" | custom-call | tf_op jit(solution)/shard_map/pallas_call | solution.py:657
  105.5 3.4 %shard_map.154 = (bf16[2048,256]{1,0:T(8,128)(2,1)}, bf16[2048,256]{1,0:T(8,128)(2,1)}, bf16[256,2048]{1,0:T(8,128)(2,1)}, bf16[64,2048]{1,0:T(8,128)(2,1)}, bf1...) custom-call(bf16[2048,256]{1,0:T(8,128)(2,1)} %get-tuple-element.21.refs_0_, ...), custom_call_target="tpu_custom_call" | custom-call | tf_op jit(solution)/shard_map/pallas_call | solution.py:632

commit v4 on v3

--- a/solution.py
+++ b/solution.py
@@ -12,7 +12,8 @@
 CORES = 2
 PARTS = 4
 VMEM_PLAN = 40 * 2**20
-VMEM_LIMIT = 60 * 2**20
+VMEM_LIMIT = 119 * 2**19
+COPY_LIMIT = 4 * 2**20
 
 
 def line_kernel(
@@ -22,8 +23,8 @@
     p_ref, gt_ref, ut_ref, dn_ref, sg_ref, su_ref, sd_ref, gain_ref, ids_ref, rw_ref,
     x_all, t_all, e_in, w_all, s_in, s_all, gate_out, up_out, acc, act, base, mixed_out,
     part, ru, rd,
-    xr, tr, er, sr, sc, fr, ur, dr,
-    zs, zd, xs, ys, xd, yd, fs_, ss, sx, sy, sd, us, ds_, loc, res_sem, in_sem,
+    xr, tr, er, sr, sc, fr, cr,
+    zs, zd, xs, ys, xd, yd, fs_, ss, sx, sy, sd, us, loc, res_sem, in_sem,
 ):
     gr, z, tp = lax.axis_index("gr"), lax.axis_index("fs"), lax.axis_index("tp")
     y, c = tp // CORES, tp % CORES
@@ -66,11 +67,11 @@
     for p in range(n_fs):
         at = pl.ds(order[p] * n_tp, n_tp)
         heavy.append([
-            pltpu.make_async_copy(src.at[at], dst.at[at], in_sem.at[1 + 3 * p + i])
-            for i, (src, dst) in enumerate(((gt_hbm, gt_ref), (ut_hbm, ut_ref), (dn_hbm, dn_ref)))
+            pltpu.make_async_copy(src.at[at], dst.at[at], in_sem.at[1 + p])
+            for src, dst in ((gt_hbm, gt_ref), (ut_hbm, ut_ref), (dn_hbm, dn_ref))
         ])
     light = [
-        pltpu.make_async_copy(src, dst, in_sem.at[1 + 3 * n_fs + i])
+        pltpu.make_async_copy(src, dst, in_sem.at[1 + n_fs + i])
         for i, (src, dst) in enumerate((
             (tsg_hbm, sg_ref), (tsu_hbm, su_ref), (tsd_hbm, sd_ref), (p_hbm, p_ref),
             (ids_hbm, ids_ref), (rw_hbm, rw_ref),
@@ -95,8 +96,8 @@
     gain = gain_ref[...]
 
     def cast(p):
-        for one in heavy[p]:
-            one.wait()
+        all_of = pl.ds(0, 3 * n_tp)
+        pltpu.make_async_copy(gt_hbm.at[all_of], gt_ref.at[all_of], in_sem.at[1 + p]).wait()
         f = order[p]
         for t in range(n_tp):
             i = f * n_tp + t
@@ -104,8 +105,10 @@
             e_in[f, t % CORES, t // CORES, 1] = (ut_ref[i] * gain).astype(jnp.bfloat16)
             e_in[f, t % CORES, t // CORES, 2] = dn_ref[i].astype(jnp.bfloat16)
 
-    cast(0)
-    pl.semaphore_wait(barrier, n_fs * CORES + 1)
+    with jax.named_scope("cast0"):
+        cast(0)
+    with jax.named_scope("greeted"):
+        pl.semaphore_wait(barrier, n_fs * CORES + 1)
 
     def remote(src, dst, send, recv, where):
         return pltpu.make_async_remote_copy(
@@ -254,7 +257,7 @@
     def half_copy(k, core, part_of):
         at = pl.ds(pl.multiple_of(part_of * half, half), half)
         place_of = w_all.at[k, core, :, :, at, :]
-        return remote(place_of, place_of, fs_.at[0], fr.at[k, part_of], to_c)
+        return remote(place_of, place_of, fs_.at[0], fr.at[k], to_c)
 
     def give(g, f, part_of):
         go(None, [half_copy(g * n_fs + f, c, part_of)], False)
@@ -306,7 +309,7 @@
         when(most, arrive)
         if most is inner:
             send_rows((f < z) & inner, f, h, 1 + p, 0)
-            send_rows((f > z) & inner, f, h, n_fs + p, 1)
+            send_rows((f > z) & inner, f, h, 1 + p, 1)
 
     def wait_shared(g, f, t):
         s_copy(None, g, f, sx.at[0], to_x, t).wait_recv()
@@ -317,7 +320,7 @@
         if p:
             when(None if most is True else most, functools.partial(wait_shared, gr, f, tp))
             go((f < z) & has_up & most, [s_copy(src, gr, f, ss.at[1 + p], up)])
-            go((f > z) & has_down & most, [s_copy(src, gr, f, ss.at[n_fs + p], down)])
+            go((f > z) & has_down & most, [s_copy(src, gr, f, ss.at[1 + p], down)])
         most = None if most is True else most
         go(most, [s_copy(src, gr, f, sx.at[0], to_x)], False)
         go(most, [s_copy(src, gr, f, sy.at[0], to_y)], False)
@@ -331,8 +334,9 @@
         return lax.dot_general(a, b, (((1,), (1,)), ((), ())), preferred_element_type=jnp.float32)
 
     def arrived(g, f):
-        for side_of in range(sides):
-            half_copy(g * n_fs + f, c_other, side_of).wait_recv()
+        k = g * n_fs + f
+        whole = w_all.at[k, c_other]
+        remote(whole, whole, fs_.at[0], fr.at[k], to_c).wait_recv()
 
     def add(k, lo, hi, first):
         at = pl.ds(pl.multiple_of(k * cols, 128), cols)
@@ -410,10 +414,11 @@
         return v.astype(jnp.float32)
 
     def u_copy(t, h):
-        return remote(part.at[t, h], ru.at[t, h], us.at[t], ur.at[t, h], up)
-
-    def d_copy(t, h):
-        return remote(part.at[t, h], rd.at[t, h], ds_.at[t], dr.at[t, h], down)
+        return remote(part.at[t, h], ru.at[t, h], us.at[t], cr.at[t, h], up)
+
+    def d_copy(t, h, last_at=None):
+        slot = jnp.where(t == (z - 1 if last_at is None else last_at), n_fs, t)
+        return remote(part.at[t, h], rd.at[t, h], us.at[t], cr.at[slot, h], down)
 
     def when_way(t, ahead, behind):
         pl.when(t > z)(ahead)
@@ -432,7 +437,7 @@
             val = jax.nn.silu(val[:, :wide_hid]) * val[:, wide_hid:] * scale
             act[s, 0:some] = val.astype(jnp.bfloat16)
 
-        group = 4
+        group = 8
 
         def columns(j, carry):
             for i in range(group):
@@ -465,7 +470,7 @@
                 @pl.when(cond)
                 def _(h=h, copy=copy, arrived=arrived):
                     with jax.named_scope("chain"):
-                        copy(t, h).wait_recv()
+                        (u_copy(t, h) if copy is u_copy else d_copy(t, h, z)).wait_recv()
                     part[t, h] = (wide(part[t, h]) + wide(arrived[t, h])).astype(jnp.bfloat16)
                     copy(t, h).start()
 
@@ -484,7 +489,7 @@
         @pl.when(has_down & has_up)
         def _():
             u_copy(z, h).wait_recv()
-            d_copy(z, h).wait_recv()
+            d_copy(z, h, z).wait_recv()
             total(ru[z, h], rd[z, h])
 
         @pl.when(jnp.logical_not(has_up))
@@ -494,7 +499,7 @@
 
         @pl.when(jnp.logical_not(has_down))
         def _():
-            d_copy(z, h).wait_recv()
+            d_copy(z, h, z).wait_recv()
             total(rd[z, h])
 
         mixed_copy(h).start()
@@ -562,33 +567,36 @@
         then(arrived, x_peer, order[p])
         then(step, x_peer, order[p], 0, 3)
     then(block, last - 1)
+    only(inner, chain, last - 1, 0, 1)
     only(inner, late, 0, parts)
+    only(inner, chain, last - 1, 1, 2)
     only(inner, block, last, 0, parts)
     for lo, hi in ((0, half_way), (half_way, parts)):
         for h in range(lo, hi):
             then(row_part, last, h, outer)
         only(outer, late, lo, hi)
         only(outer, block, last, lo, hi)
+    then(chain, last - 1, half_way, parts - 1)
     then(shared, last, inner)
-    then(chain, last - 1, 0, half_way)
     then(block, 1)
+    then(chain, last - 1, parts - 1, parts)
     then(shared, 2, outer)
     then(block, 0)
-    then(chain, last - 1, half_way, parts)
-    then(corner_turn, 2)
-    then(corner_turn, last)
     then(shared, last, outer)
     then(shared_x, 0)
     then(shared_x, 1)
-    then(chain, last, 0, half_way)
+    then(chain, last, 0, 1)
+    then(corner_turn, 2)
+    then(corner_turn, last)
+    then(chain, last, 1, 2)
     then(shared_x, 2)
     then(shared_x, last)
-    then(chain, last, half_way, parts)
-    for p in range(1, last - 1):
-        then(chain, p, 0, half_way)
+    for h in range(2, parts):
+        then(chain, 1, h - 2, h - 1)
+        then(chain, last, h, h + 1)
+    then(chain, 1, parts - 2, parts - 1)
     then(shared_give)
-    for p in range(1, last - 1):
-        then(chain, p, half_way, parts)
+    then(chain, 1, parts - 1, parts)
     then(shared_act)
     for h in range(parts):
         then(finish, h)
@@ -610,20 +618,15 @@
             when(cond, lambda copies=copies: [one.wait_send() for one in copies] and None)
         for t in range(n_fs):
             whole = part.at[t]
-            pl.when(t > z)(lambda: remote(whole, whole, us.at[t], ur.at[t, 0], up).wait_send())
-            pl.when(t < z)(lambda: remote(whole, whole, ds_.at[t], dr.at[t, 0], down).wait_send())
+            pl.when(t != z)(lambda: remote(whole, whole, us.at[t], cr.at[t, 0], to_c).wait_send())
 
 
 def copy_kernel(count, *refs):
-    ins, outs, bufs, sems = refs[:count], refs[count : 2 * count], refs[2 * count : -1], refs[-1]
-    loads = [pltpu.make_async_copy(ins[i], bufs[i], sems.at[0, i]) for i in range(count)]
-    stores = [pltpu.make_async_copy(bufs[i], outs[i], sems.at[1, i]) for i in range(count)]
-    for one in loads:
+    ins, outs, sems = refs[:count], refs[count : 2 * count], refs[-1]
+    copies = [pltpu.make_async_copy(ins[i], outs[i], sems.at[i]) for i in range(count)]
+    for one in copies:
         one.start()
-    for one, then in zip(loads, stores):
-        one.wait()
-        then.start()
-    for one in stores:
+    for one in copies:
         one.wait()
 
 
@@ -634,9 +637,8 @@
         out_shape=tuple(jax.ShapeDtypeStruct(a.shape, a.dtype) for a in arrays),
         in_specs=[pl.BlockSpec(memory_space=pl.ANY)] * count,
         out_specs=(pl.BlockSpec(memory_space=pl.ANY),) * count,
-        scratch_shapes=[pltpu.VMEM(a.shape, a.dtype) for a in arrays]
-        + [pltpu.SemaphoreType.DMA((2, count))],
-        compiler_params=pltpu.CompilerParams(vmem_limit_bytes=VMEM_LIMIT),
+        scratch_shapes=[pltpu.SemaphoreType.DMA((count,))],
+        compiler_params=pltpu.CompilerParams(vmem_limit_bytes=COPY_LIMIT),
     )(*arrays)
 
 
@@ -653,17 +655,16 @@
     f32 = jnp.float32
     hbm = pl.BlockSpec(memory_space=pl.ANY)
     dma = pltpu.SemaphoreType.DMA
-    shape = jax.ShapeDtypeStruct
     outs = pl.pallas_call(
         functools.partial(line_kernel, n_gr, n_fs, n_tp, parts),
         out_shape=(
-            shape((width, wide_hid), bf16),
-            shape((width, wide_hid), bf16),
-            shape((wide_hid, width), bf16),
-            shape((hid, width), bf16),
-            shape((hid, width), bf16),
-            shape((hid, width), bf16),
-            shape((parts, sub, width), bf16),
+            pltpu.VMEM((width, wide_hid), bf16),
+            pltpu.VMEM((width, wide_hid), bf16),
+            pltpu.VMEM((wide_hid, width), bf16),
+            pltpu.VMEM((hid, width), bf16),
+            pltpu.VMEM((hid, width), bf16),
+            pltpu.VMEM((hid, width), bf16),
+            pltpu.VMEM((parts, sub, width), bf16),
         ),
         in_specs=[hbm] * 10,
         out_specs=(hbm,) * 7,
@@ -694,11 +695,11 @@
             pltpu.VMEM((n_fs, parts, sub, width), bf16),
             pltpu.VMEM((n_fs, parts, sub, width), bf16),
             dma((n_fs, parts)), dma((n_fs,)), dma((full * n_tp,)), dma((full + 1,)),
-            dma((n_tp,)), dma((full, sides)), dma((n_fs, parts)), dma((n_fs, parts)),
-            dma((3,)), dma((2 * n_fs, 2)), dma((1,)), dma((1,)), dma((1,)), dma((1,)),
-            dma((1,)), dma((2 * n_fs,)), dma((1,)), dma((1,)), dma((2,)),
-            dma((n_fs,)), dma((n_fs,)),
-            dma((2 + parts,)), dma((6,)), dma((7 + 3 * n_fs,)),
+            dma((n_tp,)), dma((full,)), dma((n_fs + 1, parts)),
+            dma((3,)), dma((n_fs + 1, 2)), dma((1,)), dma((1,)), dma((1,)), dma((1,)),
+            dma((1,)), dma((n_fs + 1,)), dma((1,)), dma((1,)), dma((2,)),
+            dma((n_fs,)),
+            dma((2 + parts,)), dma((6,)), dma((7 + n_fs,)),
         ],
         compiler_params=pltpu.CompilerParams(
             collective_id=0, has_side_effects=True, vmem_limit_bytes=VMEM_LIMIT

time: 109 us -> 103 us (0.945)
  Pallas kernels: 108 us -> 102 us
    pallas_call x1, Pallas kernels: 105 us -> 100 us  [line_body(): pl.pallas_call(functools.partial(line_kernel, n_gr, n_fs, n_tp, parts), o...]
    pallas_call x1, Pallas kernels: 3.44 us -> 2.15 us  [copied(): pl.pallas_call(functools.partial(copy_kernel, count), out_shape=tuple((ja...]
where the time goes in v4:
time: 103 us
  Pallas kernels  102 us (99%)
    pallas_call x1, Pallas kernels, line_body(): pl.pallas_call(functools.partial(line_kernel, n_gr, n_fs, n_tp, parts), o...  100 us
    pallas_call x1, Pallas kernels, copied(): pl.pallas_call(functools.partial(copy_kernel, count), out_shape=tuple((ja...  2.15 us

profile of v4, /device:TPU:0, one launch (start us, length us, event | category | flops | bytes accessed | tf_op | source)
XLA Modules:
  0.0 102.8 jit_solution(6950565217391358796)
XLA Ops:
  0.6 100.0 %shard_map.153 = (bf16[2048,256]{1,0:T(8,128)(2,1)S(1)}, bf16[2048,256]{1,0:T(8,128)(2,1)S(1)}, bf16[256,2048]{1,0:T(8,128)(2,1)S(1)}, bf16[64,2048]{1,0:T(8,128...) custom-call(bf16[128,2048]{1,0:T(8,128)(2,1)} %p_hbm.1, ...), custom_call_target="tpu_custom_call" | custom-call | tf_op jit(solution)/shard_map/pallas_call | solution.py:658
  100.6 2.2 %shard_map.154 = (bf16[2048,256]{1,0:T(8,128)(2,1)}, bf16[2048,256]{1,0:T(8,128)(2,1)}, bf16[256,2048]{1,0:T(8,128)(2,1)}, bf16[64,2048]{1,0:T(8,128)(2,1)}, bf1...) custom-call(bf16[2048,256]{1,0:T(8,128)(2,1)S(1)} %get-tuple-element.21.refs_0_, ...), custom_call_target="tpu_custom_call" | custom-call | tf_op jit(solution)/shard_map/pallas_call | solution.py:635

commit v5 on v4

--- a/solution.py
+++ b/solution.py
@@ -61,6 +61,18 @@
         fall = jnp.where(f > at, n_fs - f, n_fs - 1 - f)
         return jnp.where(f == at, 0, jnp.where(at < n_fs // 2, rise, fall))
 
+    barrier = pltpu.get_barrier_semaphore()
+
+    def greet(where):
+        pl.semaphore_signal(barrier, inc=1, device_id=where, device_id_type=MESH)
+
+    for dz in range(n_fs):
+        for dc in range(CORES):
+            if dz or dc:
+                greet(dev(gr, (z + dz) % n_fs, y * CORES + (c + dc) % CORES))
+    greet(to_x)
+    greet(to_y)
+
     first = pltpu.make_async_copy(gain_hbm, gain_ref, in_sem.at[0])
     first.start()
     heavy = []
@@ -79,18 +91,6 @@
     ]
     for one in sum(heavy, []) + light:
         one.start()
-
-    barrier = pltpu.get_barrier_semaphore()
-
-    def greet(where):
-        pl.semaphore_signal(barrier, inc=1, device_id=where, device_id_type=MESH)
-
-    for dz in range(n_fs):
-        for dc in range(CORES):
-            if dz or dc:
-                greet(dev(gr, (z + dz) % n_fs, y * CORES + (c + dc) % CORES))
-    greet(to_x)
-    greet(to_y)
 
     first.wait()
     gain = gain_ref[...]
@@ -338,17 +338,22 @@
         whole = w_all.at[k, c_other]
         remote(whole, whole, fs_.at[0], fr.at[k], to_c).wait_recv()
 
-    def add(k, lo, hi, first):
+    def add(k, lo, hi, first, cores):
         at = pl.ds(pl.multiple_of(k * cols, 128), cols)
         lhs = x_all[lo:hi, :, :, at].reshape((hi - lo) * rows, cols)
         here = slice(lo * rows, hi * rows)
-        for s in range(n_tp):
-            w = w_all[k, s // sides, s % sides, 0:2].reshape(2 * wide_hid, cols)
-            val = nt(lhs, w)
-            acc[s, here] = val if first else acc[s, here] + val
+        for core in cores:
+            for side_of in range(sides):
+                s = core * sides + side_of
+                w = w_all[k, core, side_of, 0:2].reshape(2 * wide_hid, cols)
+                val = nt(lhs, w)
+                acc[s, here] = val if first else acc[s, here] + val
 
     def step(g, f, lo, hi, first=False):
-        add(g * n_fs + f, lo, hi, first)
+        add(g * n_fs + f, lo, hi, first, range(CORES))
+
+    def step_of(g, f, core):
+        add(g * n_fs + f, 0, n_fs - 1, False, (core,))
 
     def late(lo, hi):
         some = (hi - lo) * sub
@@ -536,8 +541,6 @@
     then(corner, 1)
     for h in range(parts):
         then(row_part, 1, h, outer)
-    then(shared, 0)
-    then(shared, 1, outer)
     then(corner_turn, 0)
     then(corner_turn, 1)
     for p in range(n_fs):
@@ -553,20 +556,22 @@
     then(step, gr, order[0], 2, 3, True)
     then(step, gr, order[1], 2, 3)
     then(corner, 2)
-    for h in range(half_way, parts - 1):
-        then(row_part, last, h, inner)
+    then(row_part, last, 2, inner)
+    then(corner, last)
     for p in range(2, n_fs):
         then(step, gr, order[p], 2, 3)
-    then(row_part, last, parts - 1, inner)
-    then(shared, 1, inner)
-    then(shared, 2, inner)
-    then(corner, last)
     for p in range(2):
         then(step, x_peer, order[p], 2, 3)
     for p in range(2, n_fs):
+        then(step_of, x_peer, order[p], c)
+    then(row_part, last, parts - 1, inner)
+    for p in range(2, n_fs):
         then(arrived, x_peer, order[p])
-        then(step, x_peer, order[p], 0, 3)
+        then(step_of, x_peer, order[p], c_other)
     then(block, last - 1)
+    then(shared, 0)
+    then(shared, 1)
+    then(shared, 2, inner)
     only(inner, chain, last - 1, 0, 1)
     only(inner, late, 0, parts)
     only(inner, chain, last - 1, 1, 2)

time: 103 us -> 102 us (level)
  no operation moved by 1% of the time
where the time goes in v5:
time: 102 us
  Pallas kernels  102 us (100%)
    pallas_call x1, Pallas kernels, line_body(): pl.pallas_call(functools.partial(line_kernel, n_gr, n_fs, n_tp, parts), o...  99.5 us
    pallas_call x1, Pallas kernels, copied(): pl.pallas_call(functools.partial(copy_kernel, count), out_shape=tuple((ja...  2.15 us

profile of v5, /device:TPU:0, one launch (start us, length us, event | category | flops | bytes accessed | tf_op | source)
XLA Modules:
  0.0 102.3 jit_solution(9869321936833210485)
XLA Ops:
  0.6 99.5 %shard_map.153 = (bf16[2048,256]{1,0:T(8,128)(2,1)S(1)}, bf16[2048,256]{1,0:T(8,128)(2,1)S(1)}, bf16[256,2048]{1,0:T(8,128)(2,1)S(1)}, bf16[64,2048]{1,0:T(8,128...) custom-call(bf16[128,2048]{1,0:T(8,128)(2,1)} %p_hbm.1, ...), custom_call_target="tpu_custom_call" | custom-call | tf_op jit(solution)/shard_map/pallas_call | solution.py:663
  100.2 2.2 %shard_map.154 = (bf16[2048,256]{1,0:T(8,128)(2,1)}, bf16[2048,256]{1,0:T(8,128)(2,1)}, bf16[256,2048]{1,0:T(8,128)(2,1)}, bf16[64,2048]{1,0:T(8,128)(2,1)}, bf1...) custom-call(bf16[2048,256]{1,0:T(8,128)(2,1)S(1)} %get-tuple-element.21.refs_0_, ...), custom_call_target="tpu_custom_call" | custom-call | tf_op jit(solution)/shard_map/pallas_call | solution.py:640
